TPU v7x, 512 devices: a whole 4x8x8 slice. The times are simulated.
512 devices in a mesh: ep: 32 (over z, x), tp: 16 (over y, core).
Axes of the slice: x: 4, y: 8, z: 8, core: 2. Of those that a mesh axis runs over, the one named last changes fastest.
Arguments:
- mixer_in: bfloat16 [4096, 2048], P('ep'), may hold values from -6 to 6
- mixer_gain: float32 [2048], replicated, may hold values from 0.1 to 1.9
- w_value: bfloat16 [2048, 1536], P(None, 'tp'), may hold values from -0.125 to 0.125
- w_gate: bfloat16 [2048, 1536], P(None, 'tp'), may hold values from -0.125 to 0.125
- w_taps: float32 [31, 1536], P(None, 'tp'), may hold values from -3 to 3
- channel_gain: float32 [1536], P('tp'), may hold values from 0.1 to 1.9
- w_output: bfloat16 [1536, 2048], P('tp'), may hold values from -0.15625 to 0.15625
- expert_in: bfloat16 [4096, 2048], P('ep'), may hold values from -6 to 6
- expert_gain: float32 [2048], replicated, may hold values from 0 to 8
- route_experts: int32 [4096, 4], P('ep'), may hold values from 0 to 31, all different within a row; in each aligned block of 128 rows (0 to 127, 128 to 255, ...) at most 32 rows name the same one
- route_scores: float32 [4096, 4], P('ep'), may hold values from -6 to 6
- expert_gate: bfloat16 [32, 2048, 2048], P('ep', None, 'tp'), may hold values from -0.125 to 0.125
- expert_up: bfloat16 [32, 2048, 2048], P('ep', None, 'tp'), may hold values from -0.125 to 0.125
- expert_down: bfloat16 [32, 2048, 2048], P('ep', 'tp'), may hold values from -0.125 to 0.125
Outputs:
- mixer_out: bfloat16 [4096, 2048], P('ep')
- expert_out: bfloat16 [4096, 2048], P('ep')
Inputs may be any that keep to these rules, and one draw needn't show every extreme that they name: `route_experts`: each row names 4 different experts. In each aligned block of 128 rows (the rows of one index of ep) no expert is named more than 32 times, a bound that some block reaches.
All inputs are finite; a program needn't handle non-finite values.
Results may differ from a plain program's by a relative error of at most 0.02.
Values may be sent and summed in bfloat16 or wider, within the bound.
A program may use at most 64 MiB of HBM per device.

v0:
```python
import jax
import jax.numpy as jnp
from jax import lax
from jax.sharding import Mesh
from jax.sharding import PartitionSpec as P

CONV_CH = 1536
CONV_W = 31
TOP_K = 4
TP = ("tp_0", "tp_1")


epsilon = 1e-05
clamp_limit = 7.0
swish_slope = 1.702


def shifted(block, axis, distance):
    devices = range(lax.axis_size(axis))
    route = [(i - distance, i) for i in devices if i - distance in devices]
    return lax.ppermute(block, axis, route)


def sent_to_all(x, axis):
    copies = jnp.broadcast_to(x, (lax.axis_size(axis), *x.shape))
    return lax.all_to_all(copies, axis, split_axis=0, concat_axis=0, tiled=True)


def over_copies(x, axis):
    everything = sent_to_all(x, axis)
    return jnp.sum(everything, axis=0)


def packed_total(arrays, axis):
    line, at, done = (jnp.concatenate([a.reshape(-1) for a in arrays]), 0, [])
    subtotal = over_copies(line, axis)
    for a in arrays:
        done.append(subtotal[at : at + a.size].reshape(a.shape))
        at += a.size
    return tuple(done)


def by_axis(x, axes):
    for axis in axes:
        x = lax.psum(x, axis)
    return x


def row_norm(inputs, gains):
    widened = inputs.astype(jnp.float32)
    row_mean = jnp.mean(widened, axis=-1, keepdims=True)
    row_var = jnp.mean(jnp.square(widened - row_mean), axis=-1, keepdims=True)
    return (widened - row_mean) * lax.rsqrt(row_var + epsilon) * gains


def local(
    mixer_in,
    mixer_gain,
    w_value,
    w_gate,
    w_taps,
    channel_gain,
    w_output,
    expert_in,
    expert_gain,
    route_experts,
    route_scores,
    expert_gate,
    expert_up,
    expert_down,
):
    normed = row_norm(mixer_in, mixer_gain).astype(jnp.bfloat16)
    values = jnp.dot(normed, w_value, preferred_element_type=jnp.float32)
    gate_pre = jnp.dot(normed, w_gate, preferred_element_type=jnp.float32)
    gated_values = (values * jax.nn.sigmoid(gate_pre)).astype(jnp.bfloat16)
    mixer_rows = gated_values.shape[0]
    reach_rows = CONV_W - 1
    earlier = shifted(gated_values[mixer_rows - reach_rows :], "ep", 1)
    extended = jnp.concatenate([earlier, gated_values], axis=0)
    conv_out = jnp.zeros(gated_values.shape, jnp.float32)
    for offset in range(CONV_W):
        conv_out = (
            conv_out + extended[offset : offset + mixer_rows].astype(jnp.float32) * w_taps[offset]
        )
    channel_sums = packed_total(
        (
            jnp.sum(conv_out, axis=1, keepdims=True),
            jnp.sum(conv_out * conv_out, axis=1, keepdims=True),
        ),
        TP,
    )
    row_mean = channel_sums[0] / CONV_CH
    row_var = channel_sums[1] / CONV_CH - row_mean * row_mean
    activated = jax.nn.silu(
        (conv_out - row_mean) * lax.rsqrt(row_var + epsilon) * channel_gain
    ).astype(jnp.bfloat16)
    mixer_out = (
        by_axis(
            jnp.dot(activated, w_output, preferred_element_type=jnp.float32).astype(jnp.bfloat16),
            TP,
        )
        .astype(jnp.float32)
        .astype(jnp.bfloat16)
    )
    rows_b = expert_in.shape[0]
    width = expert_in.shape[1]
    experts = lax.axis_size("ep")
    capacity = 2 * rows_b * TOP_K // experts
    slot_share = capacity // lax.axis_size(TP)
    column = lax.axis_index(TP)
    normed_b = row_norm(expert_in, expert_gain).astype(jnp.bfloat16)
    raised = jnp.exp(route_scores)
    route_weights = raised / jnp.sum(raised, axis=1, keepdims=True)
    flat_ids = route_experts.reshape(-1)
    onehot = (flat_ids[:, None] == jnp.arange(experts, dtype=jnp.int32)[None, :]).astype(jnp.int32)
    slot_index = jnp.sum((jnp.cumsum(onehot, axis=0) - onehot) * onehot, axis=1)
    owner_row = jnp.arange(rows_b * TOP_K, dtype=jnp.int32) // TOP_K
    slot_table = (
        jnp.full((capacity * experts,), rows_b, jnp.int32)
        .at[slot_index * experts + flat_ids]
        .set(owner_row)
    )
    padded = jnp.concatenate([normed_b, jnp.zeros((1, width), jnp.bfloat16)], axis=0)
    gate_w = expert_gate[0]
    up_w = expert_up[0]
    down_w = expert_down[0]
    own_table = lax.dynamic_slice_in_dim(
        slot_table, column * slot_share * experts, slot_share * experts
    )
    sending = jnp.take(padded, own_table, axis=0).reshape(slot_share, experts, width)
    arrived = lax.all_to_all(sending, "ep", split_axis=1, concat_axis=1, tiled=True)
    block_rows = lax.all_gather(arrived, TP, axis=0, tiled=True)
    flat_rows = block_rows.reshape(block_rows.shape[0] * block_rows.shape[1], block_rows.shape[2])
    gate_e = jnp.minimum(
        jnp.dot(flat_rows, gate_w, preferred_element_type=jnp.float32), clamp_limit
    )
    up_e = jnp.clip(
        jnp.dot(flat_rows, up_w, preferred_element_type=jnp.float32), -clamp_limit, clamp_limit
    )
    hidden = (
        ((up_e + 1.0) * gate_e * jax.nn.sigmoid(swish_slope * gate_e))
        .astype(jnp.bfloat16)
        .reshape(block_rows.shape[0], block_rows.shape[1], gate_w.shape[1])
        .reshape(capacity * experts, gate_w.shape[1])
    )
    summed = lax.psum_scatter(
        jnp.dot(hidden, down_w, preferred_element_type=jnp.float32).astype(jnp.bfloat16),
        TP,
        scatter_dimension=0,
        tiled=True,
    )
    returned = lax.all_to_all(
        summed.reshape(slot_share, experts, width), "ep", split_axis=1, concat_axis=1, tiled=True
    )
    every_slot = lax.all_gather(returned, TP, axis=0, tiled=True).reshape(capacity * experts, width)
    picked = jnp.take(every_slot, slot_index * experts + flat_ids, axis=0)
    picked = picked.reshape(rows_b, TOP_K, width).astype(jnp.float32)
    expert_out = jnp.sum(picked * route_weights[:, :, None], axis=1).astype(jnp.bfloat16)
    return (mixer_out, expert_out)


def solution(mesh):
    split = Mesh(mesh.devices.reshape(mesh.shape["ep"], 8, 2), ("ep", "tp_0", "tp_1"))
    in_specs = (
        P("ep", None),
        P(),
        P(None, TP),
        P(None, TP),
        P(None, TP),
        P(TP),
        P(TP, None),
        P("ep", None),
        P(),
        P("ep", None),
        P("ep", None),
        P("ep", None, TP),
        P("ep", None, TP),
        P("ep", TP, None),
    )
    out_specs = (P("ep", None), P("ep", None))
    return jax.shard_map(local, mesh=split, in_specs=in_specs, out_specs=out_specs, check_vma=False)
```

profile of v0, /device:TPU:1, one launch (start us, length us, event | category | flops | bytes accessed | tf_op | source)
XLA Modules:
  0.0 251.4 jit_solution(10205323536202366580)
XLA Ops:
  8.1 0.9 copy.59
  9.0 0.1 eq.29
  9.1 0.1 eq.25
  9.2 0.1 reshape.133
  9.3 1.2 reduce-window.6
  10.5 0.2 slice_reduce_fusion
  10.7 0.1 fusion.34
  10.9 2.4 scatter_custom_fusion
  13.3 0.1 compare_and_fusion
  13.4 1.2 convert_reduce_fusion
  14.6 1.3 fusion.13
  16.0 0.1 broadcast_in_dim.45
  16.1 0.1 copy.65
  16.2 1.4 fusion.15
  17.6 0.7 gather_fusion
  18.4 0.3 broadcast_select_fusion
  18.7 24.8 %all_to_all.16 = bf16[2,32,2048]{2,0,1:T(2,128)(2,1)S(1)} all-to-all(bf16[2,32,2048]{2,0,1:T(2,128)(2,1)S(1)} %broadcast_select_fusion), channel_id=1, replica_groups=mesh['ep'=32,'tp_0'=8,'tp_1'=2] {'ep'}, dimensions={1} | all-to-all | bytes 524288 | tf_op jit(solution)/shard_map/all_to_all | solution.py:131
  43.6 0.8 copy.67
  44.4 42.1 %all-gather.3.cloned.1.call-done = bf16[32,32,2048]{2,1,0:T(8,128)(2,1)} async-done(((bf16[2,32,2048]{2,1,0:T(8,128)(2,1)}), bf16[32,32,2048]{2,1,0:T(8,128)(2,1)}) %all-gather.3.cloned.1.call-update) | async-done | bytes 4194320 | tf_op jit(solution)/shard_map/all_gather | solution.py:132
  86.5 3.4 %convolution_minimum_fusion = f32[1024,128]{1,0:T(8,128)S(1)} fusion(bf16[1024,2048]{1,0:T(8,128)(2,1)} %bitcast.103, bf16[1,2048,128]{2,1,0:T(8,128)(2,1)S(1)} %copy-done.8), kind=kOutput, calls=%fused_computation.14 | convolution fusion | flops 537001984 | bytes 5242880 | tf_op jit(solution)/shard_map/dot_general | solution.py:135
  90.0 8.5 %convolution_convert_fusion = bf16[1024,2048]{1,0:T(8,128)(2,1)} fusion(f32[1024,128]{1,0:T(8,128)S(1)} %convolution_minimum_fusion, bf16[1024,2048]{1,0:T(8,128)(2,1)} %bitcast.104, bf16[1,128,2048]{2,1,0:T(8,128)(2,1)S(1)} %copy-done, bf16[1,2048,128]{2,1,0:T(8,128)(2,1)S(1)} %copy-done.2), kind=kOutput, calls=%fused_computation.4 | convolution fusion | flops 1077018624 | bytes 9961472 | tf_op jit(solution)/shard_map/dot_general | solution.py:147
  98.6 0.0 all-reduce.4.cloned.1.call-start
  98.6 0.9 copy-done.1
  99.5 0.2 convert_reduce_fusion.1
  99.7 0.3 fusion.16
  100.0 0.4 fusion.80
  100.4 0.4 fusion.12
  100.8 0.1 slice.268
  100.9 3.1 %collective-permute-start = (bf16[30,96]{0,1:T(8,128)(2,1)S(1)}, bf16[30,96]{0,1:T(8,128)(2,1)S(1)}, u32[]{:S(2)}, u32[]{:S(2)}) collective-permute-start(bf16[30,96]{0,1:T(8,128)(2,1)S(1)} %slice.268), channel_id=1, source_target_pairs={{0,16},{16,32},{32,48},{48,64},{64,80},{80,96},{96,112},{112,128},... | collective-permute-start | bytes 17288 | tf_op jit(solution)/shard_map/ppermute | solution.py:21
  104.1 0.9 collective-permute-done
  104.9 0.9 fusion.82
  105.8 12.5 %all_to_all.17 = f32[16,1,256]{2,1,0:T(1,128)S(1)} all-to-all(f32[16,1,256]{2,1,0:T(1,128)S(1)} %broadcast_in_dim.42), channel_id=1, replica_groups=mesh['ep'=32,'tp_0'=8,'tp_1'=2] {'tp_0','tp_1'}, dimensions={0} | all-to-all | bytes 32768 | tf_op jit(solution)/shard_map/all_to_all | solution.py:26
  118.4 1.2 convolution_convert_fusion.1
  119.6 42.9 %reduce-scatter.2.cloned.1.call-done = bf16[64,2048]{1,0:T(8,128)(2,1)} async-done(((bf16[1024,2048]{1,0:T(8,128)(2,1)}), bf16[64,2048]{1,0:T(8,128)(2,1)}) %reduce-scatter.2.cloned.1.call-update) | async-done | bytes 262160 | tf_op jit(solution)/shard_map/reduce_scatter | solution.py:146
  162.5 1.2 copy.68
  163.8 18.9 %all_to_all.18 = bf16[2,32,2048]{2,0,1:T(2,128)(2,1)S(1)} all-to-all(bf16[2,32,2048]{2,0,1:T(2,128)(2,1)S(1)} %copy.68), channel_id=1, replica_groups=mesh['ep'=32,'tp_0'=8,'tp_1'=2] {'ep'}, dimensions={1} | all-to-all | bytes 524288 | tf_op jit(solution)/shard_map/all_to_all | solution.py:152
  182.7 0.8 copy.69
  183.5 0.2 all-reduce.6.cloned.1.call-start
  183.7 0.1 mul.529
  183.8 0.1 copy.62
  183.9 0.1 copy.63
  184.1 0.1 copy.70
  184.2 9.5 %all-reduce.4.cloned.1.call-done = bf16[128,2048]{1,0:T(8,128)(2,1)} async-done(((bf16[128,2048]{1,0:T(8,128)(2,1)}), bf16[128,2048]{1,0:T(8,128)(2,1)}) %all-reduce.4.cloned.1.call-update) | async-done | bytes 524304 | tf_op jit(solution)/shard_map/psum | solution.py:45
  193.8 32.8 %all-gather.5.cloned.1.call-done = bf16[32,32,2048]{2,1,0:T(8,128)(2,1)} async-done(((bf16[2,32,2048]{2,1,0:T(8,128)(2,1)}), bf16[32,32,2048]{2,1,0:T(8,128)(2,1)}) %all-gather.5.cloned.1.call-update) | async-done | bytes 4194320 | tf_op jit(solution)/shard_map/all_gather | solution.py:155
  226.6 7.1 %gather_fusion.1 = bf16[512,2048]{1,0:T(8,128)(2,1)S(1)} fusion(bf16[1024,2048]{1,0:T(8,128)(2,1)} %bitcast.102, s32[1024]{0:T(1024)S(1)} %pad_clamp_fusion), kind=kCustom, calls=%fused_computation.1 | custom fusion | bytes 4196352 | tf_op jit(solution)/shard_map/jit(_take)/gather | solution.py:156
  233.7 2.2 gather.15
  236.0 6.4 %multiply_reduce_fusion = bf16[128,2048]{1,0:T(8,128)(2,1)} fusion(f32[128,4]{1,0:T(8,128)S(1)} %copy.70, bf16[128,4,2048]{2,1,0:T(4,128)(2,1)} %gather.15, pred[128,4]{1,0:T(8,128)(4,1)S(1)} %copy.63), kind=kLoop, calls=%fused_computation.3 | loop fusion | flops 3932160 | bytes 2624000 | tf_op jit(solution)/shard_map/reduce_sum | solution.py:158
  242.4 1.9 copy.79
  (54 shorter events, 0.6 us)
Async XLA Ops:
  8.0 82.0 %copy-start = (bf16[1,128,2048]{2,1,0:T(8,128)(2,1)S(1)}, bf16[1,128,2048]{2,1,0:T(8,128)(2,1)}, u32[]{:S(2)}) copy-start(bf16[1,128,2048]{2,1,0:T(8,128)(2,1)} %param.27) | copy-start | bytes 1572868
  8.0 78.5 %copy-start.8 = (bf16[1,2048,128]{2,1,0:T(8,128)(2,1)S(1)}, bf16[1,2048,128]{2,1,0:T(8,128)(2,1)}, u32[]{:S(2)}) copy-start(bf16[1,2048,128]{2,1,0:T(8,128)(2,1)} %param.25) | copy-start | bytes 1572868
  8.0 78.5 %all-gather.3.cloned.1.call-start = ((), (), s32[]{:S(2)}) async-start(), calls=%async_computation.6 | async-start | bytes 4456448 | tf_op jit(solution)/shard_map/all_gather | solution.py:132
  18.4 71.6 %copy-start.2 = (bf16[1,2048,128]{2,1,0:T(8,128)(2,1)S(1)}, bf16[1,2048,128]{2,1,0:T(8,128)(2,1)}, u32[]{:S(2)}) copy-start(bf16[1,2048,128]{2,1,0:T(8,128)(2,1)} %param.26) | copy-start | bytes 1572868
  44.4 118.2 %reduce-scatter.2.cloned.1.call-start = ((), (), s32[]{:S(2)}) async-start(), calls=%async_computation.7 | async-start | bytes 4456448 | tf_op jit(solution)/shard_map/reduce_scatter | solution.py:146
  98.5 1.0 copy-start.1
  98.5 1.5 copy-start.9
  98.5 1.5 copy-start.11
  98.5 1.9 copy-start.10
  98.5 5.5 %copy-start.4 = (f32[31,96]{1,0:T(8,128)S(1)}, f32[31,96]{1,0:T(8,128)}, u32[]{:S(2)}) copy-start(f32[31,96]{1,0:T(8,128)} %param.18) | copy-start | bytes 35716
  98.5 19.9 %copy-start.3 = (bf16[96,2048]{1,0:T(8,128)(2,1)S(1)}, bf16[96,2048]{1,0:T(8,128)(2,1)}, u32[]{:S(2)}) copy-start(bf16[96,2048]{1,0:T(8,128)(2,1)} %param.20) | copy-start | bytes 1179652
  98.5 19.8 %copy-start.7 = (f32[96]{0:T(128)S(1)}, f32[96]{0:T(128)}, u32[]{:S(2)}) copy-start(f32[96]{0:T(128)} %param.19) | copy-start | bytes 1156
  98.5 85.3 %copy-start.5 = (s32[128,4]{0,1:T(4,128)S(1)}, s32[128,4]{0,1:T(4,128)}, u32[]{:S(2)}) copy-start(s32[128,4]{0,1:T(4,128)} %param.23) | copy-start | bytes 6148
  98.6 85.5 %copy-start.6 = (f32[128,4]{0,1:T(4,128)S(1)}, f32[128,4]{0,1:T(4,128)}, u32[]{:S(2)}) copy-start(f32[128,4]{0,1:T(4,128)} %param.24) | copy-start | bytes 6148
  98.6 95.1 %all-reduce.4.cloned.1.call-start = ((), (), s32[]{:S(2)}) async-start(), calls=%async_computation.4 | async-start | bytes 1048576 | tf_op jit(solution)/shard_map/psum | solution.py:45
  100.9 4.0 %collective-permute-start = (bf16[30,96]{0,1:T(8,128)(2,1)S(1)}, bf16[30,96]{0,1:T(8,128)(2,1)S(1)}, u32[]{:S(2)}, u32[]{:S(2)}) collective-permute-start(bf16[30,96]{0,1:T(8,128)(2,1)S(1)} %slice.268), channel_id=1, source_target_pairs={{0,16},{16,32},{32,48},{48,64},{64,80},{80,96},{96,112},{112,128},... | collective-permute-start | bytes 17288 | tf_op jit(solution)/shard_map/ppermute | solution.py:21
  119.6 107.0 %all-gather.5.cloned.1.call-start = ((), (), s32[]{:S(2)}) async-start(), calls=%async_computation.8 | async-start | bytes 4456448 | tf_op jit(solution)/shard_map/all_gather | solution.py:155
  183.5 58.9 %all-reduce.6.cloned.1.call-start = ((), (), s32[]{:S(2)}) async-start(), calls=%async_computation.5 | async-start | bytes 1048576 | tf_op jit(solution)/shard_map/psum | solution.py:45
Sparse Core Ops, SparseCore 0:
  44.5 42.0 all-gather.2
  98.7 63.8 reduce-scatter.1
  183.6 42.9 all-gather.4
Sparse Core Ops, SparseCore 1:
  119.7 74.0 all-reduce.3
  196.5 39.0 all-reduce.5
where the time goes:
time: 252 us; the launch traced here: 251 us
  waiting for transfers between devices  128 us (51%)
  blocking collectives  56.2 us (22%)
  local copies, waits for them, and re-layouts  20.4 us (8%)
  between operations  15.5 us (6%)
  matrix products  13.9 us (6%)
  other arithmetic  13.6 us (5%)
  starting transfers between devices  3.48 us (1%)
    reduce_scatter x1, waiting for transfers between devices, local(): lax.psum_scatter(jnp.dot(hidden, down_w, preferred_element_type=jnp.float...  42.9 us
    all_gather x1, waiting for transfers between devices, local(): block_rows = lax.all_gather(arrived, TP, axis=0, tiled=True)  42.1 us
    all_gather x1, waiting for transfers between devices, local(): lax.all_gather(returned, TP, axis=0, tiled=True)  32.8 us
    all_to_all x1, blocking collectives, local(): lax.all_to_all(sending, 'ep', split_axis=1, concat_axis=1, tiled=True)  24.8 us
    all_to_all x1, blocking collectives, local(): lax.all_to_all(summed.reshape(slot_share, experts, width), 'ep', split_ax...  18.9 us
    all_to_all x1, blocking collectives, sent_to_all(): return lax.all_to_all(copies, axis, split_axis=0, concat_axis=0, tiled=True)  12.5 us
    psum x2, waiting for transfers between devices, by_axis(): x = lax.psum(x, axis)  9.51 us
    gather x2, local copies, waits for them, and re-layouts, local(): picked = jnp.take(every_slot, slot_index * experts + flat_ids, axis=0)  9.37 us
  transfers between devices with their start and end apart: 6, of which 5 were waited for; matrix products, arithmetic and copies ran while one was open for 9% of the time, Pallas kernels for 0%

commit v1 on v0

v1 whole, which is shorter than its diff:
```python
import functools

import jax
import jax.numpy as jnp
from jax import lax
from jax.experimental import pallas as pl
from jax.experimental.pallas import tpu as pltpu
from jax.sharding import Mesh
from jax.sharding import PartitionSpec as P

CONV_CH = 1536
CONV_W = 31
EP = ("z", "x")
TP = ("y", "c")
NZ, NX, NY = 8, 4, 8
SLOTS = 32
FAR = NY // 2

epsilon = 1e-05
clamp_limit = 7.0
swish_slope = 1.702

VM = pl.BlockSpec(memory_space=pltpu.VMEM)
ANY = pl.BlockSpec(memory_space=pl.ANY)
DMA = pltpu.SemaphoreType.DMA


def shift_of(y, c, j):
    m = 2 * c + j
    return (2 * m + 1 - y // 4) % NZ, (y % 4 + m) % NX


def reach(way, j):
    return FAR if way == j else FAR - 1


def put(src, dst, sent, landed, **device):
    return pltpu.make_async_remote_copy(
        src_ref=src,
        dst_ref=dst,
        send_sem=sent,
        recv_sem=landed,
        device_id=device,
        device_id_type=pl.DeviceIdType.MESH,
    )


def greet(barrier, **device):
    pl.semaphore_signal(barrier, inc=1, device_id=device, device_id_type=pl.DeviceIdType.MESH)


def place():
    return tuple(lax.axis_index(a) for a in ("z", "x", "y", "c"))


def greet_shifts(barrier, z, x, y, c):
    itself = jnp.logical_and(y == 4, c == 0)
    for j in range(2):
        dz, dx = shift_of(y, c, j)

        def both():
            greet(barrier, z=(z + dz) % NZ, x=(x + dx) % NX)
            greet(barrier, z=(z + NZ - dz) % NZ, x=(x + NX - dx) % NX)

        if j == 0:
            pl.when(jnp.logical_not(itself))(both)
        else:
            both()
    return itself


def wait_greets(barrier, itself, others):
    pl.semaphore_wait(barrier, jnp.where(itself, others + 2, others + 4))


def dispatch_kernel(
    send, halo_in, gate_hbm, up_hbm, hidden, halo_out, rows, weights,
    w_sem, a_sent, a_here, local_sem, h_sent, h_here, hop_sent, hop_here,
    own_sent, own_here, rel_sent, rel_here,
):
    z, x, y, c = place()
    other = 1 - c
    sides = ((y + 1) % NY, (y + NY - 1) % NY)
    block = z * NX + x
    after = (block + 1) % (NZ * NX)
    before = (block + NZ * NX - 1) % (NZ * NX)

    barrier = pltpu.get_barrier_semaphore()
    itself = greet_shifts(barrier, z, x, y, c)
    greet(barrier, y=sides[0])
    greet(barrier, y=sides[1])
    greet(barrier, c=other)
    greet(barrier, z=after // NX, x=after % NX)
    greet(barrier, z=before // NX, x=before % NX)
    gate_copy = pltpu.make_async_copy(gate_hbm.at[0], weights.at[:, pl.ds(0, 128)], w_sem.at[0])
    up_copy = pltpu.make_async_copy(up_hbm.at[0], weights.at[:, pl.ds(128, 128)], w_sem.at[1])
    gate_copy.start()
    up_copy.start()
    wait_greets(barrier, itself, 5)

    def shifted(j):
        dz, dx = shift_of(y, c, j)
        return put(
            send.at[j], rows.at[c, y, j], a_sent.at[j], a_here.at[j],
            z=(z + dz) % NZ, x=(x + dx) % NX,
        )

    stays = pltpu.make_async_copy(send.at[0], rows.at[c, y, 0], local_sem)

    @pl.when(itself)
    def _():
        stays.start()

    @pl.when(jnp.logical_not(itself))
    def _():
        shifted(0).start()

    shifted(1).start()
    halo = put(halo_in, halo_out, h_sent, h_here, z=after // NX, x=after % NX)
    halo.start()

    def origin(k, way):
        return (y + NY - k) % NY if way == 0 else (y + k) % NY

    def hop(k, j, way):
        piece = rows.at[c, origin(k, way), j]
        return put(piece, piece, hop_sent.at[way, k, j], hop_here.at[way, k, j], y=sides[way])

    def own(j):
        piece = rows.at[c, y, j]
        return put(piece, piece, own_sent.at[j], own_here.at[j], c=other)

    def relay(k, j, way):
        piece = rows.at[c, origin(k + 1, way), j]
        return put(piece, piece, rel_sent.at[way, k, j], rel_here.at[way, k, j], c=other)

    def product(core, source):
        inputs = rows[core, source].reshape(2 * SLOTS, 2048)
        both = jnp.dot(inputs, weights[...], preferred_element_type=jnp.float32)
        gate = jnp.minimum(both[:, :128], clamp_limit)
        up = jnp.clip(both[:, 128:], -clamp_limit, clamp_limit)
        hidden[core, source] = (
            (up + 1.0) * gate * jax.nn.sigmoid(swish_slope * gate)
        ).astype(jnp.bfloat16)

    for j in range(2):
        if j == 0:

            @pl.when(itself)
            def _():
                stays.wait()

            @pl.when(jnp.logical_not(itself))
            def _():
                shifted(0).wait()
        else:
            shifted(1).wait()
        for way in range(2):
            hop(0, j, way).start()
        own(j).start()
    gate_copy.wait()
    up_copy.wait()
    product(c, y)
    for j in range(2):
        own(j).wait()
    product(other, y)
    for k in range(FAR):
        for j in range(2):
            for way in range(2):
                if k < reach(way, j):
                    hop(k, j, way).wait_recv()
                    if k + 1 < reach(way, j):
                        hop(k + 1, j, way).start()
                    relay(k, j, way).start()
        ways = (0, 1) if k < FAR - 1 else (0,)
        for way in ways:
            product(c, origin(k + 1, way))
        for j in range(2):
            for way in range(2):
                if k < reach(way, j):
                    relay(k, j, way).wait_recv()
        for way in ways:
            product(other, origin(k + 1, way))
    halo.wait()
    for k in range(FAR):
        for j in range(2):
            for way in range(2):
                if k < reach(way, j):
                    hop(k, j, way).wait_send()
                    relay(k, j, way).wait_send()


def dispatch(send, halo_in, gate_w, up_w):
    return pl.pallas_call(
        dispatch_kernel,
        out_shape=(
            jax.ShapeDtypeStruct((2, NY, 2 * SLOTS, 128), jnp.bfloat16),
            jax.ShapeDtypeStruct((32, 128), jnp.bfloat16),
        ),
        in_specs=[VM, VM, ANY, ANY],
        out_specs=(VM, VM),
        scratch_shapes=[
            pltpu.VMEM((2, NY, 2, SLOTS, 2048), jnp.bfloat16),
            pltpu.VMEM((2048, 256), jnp.bfloat16),
            DMA((2,)),
            DMA((2,)),
            DMA((2,)),
            DMA,
            DMA,
            DMA,
            DMA((2, FAR, 2)),
            DMA((2, FAR, 2)),
            DMA((2,)),
            DMA((2,)),
            DMA((2, FAR, 2)),
            DMA((2, FAR, 2)),
        ],
        compiler_params=pltpu.CompilerParams(
            collective_id=0, has_side_effects=True, vmem_limit_bytes=24 << 20
        ),
        name="dispatch",
    )(send, halo_in, gate_w, up_w)


def combine_kernel(
    hidden, down, stats, returned, stats_out, given, taken, chain_in, chain_out, mine,
    final, pair, pair_sum, stats_all, give_sent, give_here, hop_sent, hop_here, r_sent, r_here,
    local_sem, p_sent, p_here, s_sent, s_here,
):
    z, x, y, c = place()
    other = 1 - c
    sides = ((y + 1) % NY, (y + NY - 1) % NY)
    barrier = pltpu.get_barrier_semaphore()
    itself = greet_shifts(barrier, z, x, y, c)
    greet(barrier, c=other)
    for i in range(1, NY):
        greet(barrier, y=(y + i) % NY)

    def away(m, way):
        return (y + m) % NY if way == 0 else (y + NY - m) % NY

    order = [(FAR, 0)] + [(m, way) for m in range(FAR - 1, 0, -1) for way in range(2)] + [(0, 0)]

    def gift(i):
        dest = away(*order[i])
        return put(given.at[dest], taken.at[dest], give_sent.at[i], give_here.at[i], c=other)

    def give(i):
        dest = away(*order[i])

        def columns(n, _):
            at = pl.ds(pl.multiple_of(n * 512, 512), 512)
            given[dest, :, at] = jnp.dot(
                hidden[other, dest], down[0, :, at], preferred_element_type=jnp.float32
            ).astype(jnp.bfloat16)
            return 0

        lax.fori_loop(0, 4, columns, 0)
        gift(i).start()

    def add_up(i, slot):
        dest = away(*order[i])
        gift(i).wait_recv()

        def columns(n, _):
            at = pl.ds(pl.multiple_of(n * 512, 512), 512)
            mine[slot, :, at] = jnp.dot(
                hidden[c, dest], down[0, :, at], preferred_element_type=jnp.float32
            ) + taken[dest, :, at].astype(jnp.float32)
            return 0

        lax.fori_loop(0, 4, columns, 0)

    def hop(m, j, way):
        return put(
            chain_out.at[way, m - 1, j], chain_in.at[way, m - 1, j],
            hop_sent.at[way, m - 1, j], hop_here.at[way, m - 1, j], y=sides[way],
        )

    def pass_on(m, j, way, slot):
        total = mine[slot, j * SLOTS : (j + 1) * SLOTS]
        if m < reach(way, j):
            hop(m + 1, j, way).wait_recv()
            total = total + chain_in[way, m, j].astype(jnp.float32)
        chain_out[way, m - 1, j] = total.astype(jnp.bfloat16)
        hop(m, j, way).start()

    def swap():
        return put(stats, pair, p_sent, p_here, c=other)

    def spread(i):
        return put(
            pair_sum, stats_all.at[y], s_sent.at[i], s_here.at[i], y=(y + i) % NY
        )

    dest = away(*order[0])

    def first(n, _):
        at = pl.ds(pl.multiple_of(n * 512, 512), 512)
        given[dest, :, at] = jnp.dot(
            hidden[other, dest], down[0, :, at], preferred_element_type=jnp.float32
        ).astype(jnp.bfloat16)
        return 0

    lax.fori_loop(0, 4, first, 0)
    wait_greets(barrier, itself, NY)
    gift(0).start()
    swap().start()
    give(1)
    give(2)
    add_up(0, 0)
    pass_on(FAR, 0, 0, 0)
    pass_on(FAR, 1, 1, 0)
    for m in range(FAR - 1, 0, -1):
        i = 1 + 2 * (FAR - 1 - m)
        give(i + 2)
        if m > 1:
            give(i + 3)
        add_up(i, 0)
        add_up(i + 1, 1)
        for turn in range(2):
            for way in range(2):
                pass_on(m, 1 - way if turn == 0 else way, way, way)
        if m == FAR - 1:
            swap().wait()
            pair_sum[...] = stats[...] + pair[...]
            for i in range(1, NY):
                spread(i).start()
    add_up(len(order) - 1, 0)
    total = pair_sum[...]
    for i in range(1, NY):
        spread(i).wait()
        total = total + stats_all[(y + NY - i) % NY]
    stats_out[...] = total

    def goes_back(j):
        dz, dx = shift_of(y, c, j)
        return put(
            final.at[j], returned.at[j], r_sent.at[j], r_here.at[j],
            z=(z + NZ - dz) % NZ, x=(x + NX - dx) % NX,
        )

    stays = pltpu.make_async_copy(final.at[0], returned.at[0], local_sem)
    for j in range(2):
        hop(1, j, 0).wait_recv()
        hop(1, j, 1).wait_recv()
        final[j] = (
            mine[0, j * SLOTS : (j + 1) * SLOTS]
            + chain_in[0, 0, j].astype(jnp.float32)
            + chain_in[1, 0, j].astype(jnp.float32)
        ).astype(jnp.bfloat16)
        if j == 0:

            @pl.when(itself)
            def _():
                stays.start()

            @pl.when(jnp.logical_not(itself))
            def _():
                goes_back(0).start()
        else:
            goes_back(1).start()
    for i in range(len(order)):
        gift(i).wait_send()
    for m in range(1, FAR + 1):
        for j in range(2):
            for way in range(2):
                if m <= reach(way, j):
                    hop(m, j, way).wait_send()

    @pl.when(itself)
    def _():
        stays.wait()

    @pl.when(jnp.logical_not(itself))
    def _():
        goes_back(0).wait()

    goes_back(1).wait()


def combine(hidden, down_w, stats):
    return pl.pallas_call(
        combine_kernel,
        out_shape=(
            jax.ShapeDtypeStruct((2, SLOTS, 2048), jnp.bfloat16),
            jax.ShapeDtypeStruct((8, 128), jnp.float32),
        ),
        in_specs=[VM, VM, VM],
        out_specs=(VM, VM),
        scratch_shapes=[
            pltpu.VMEM((NY, 2 * SLOTS, 2048), jnp.bfloat16),
            pltpu.VMEM((NY, 2 * SLOTS, 2048), jnp.bfloat16),
            pltpu.VMEM((2, FAR, 2, SLOTS, 2048), jnp.bfloat16),
            pltpu.VMEM((2, FAR, 2, SLOTS, 2048), jnp.bfloat16),
            pltpu.VMEM((2, 2 * SLOTS, 2048), jnp.float32),
            pltpu.VMEM((2, SLOTS, 2048), jnp.bfloat16),
            pltpu.VMEM((8, 128), jnp.float32),
            pltpu.VMEM((8, 128), jnp.float32),
            pltpu.VMEM((NY, 8, 128), jnp.float32),
            DMA((2 * FAR,)),
            DMA((2 * FAR,)),
            DMA((2, FAR, 2)),
            DMA((2, FAR, 2)),
            DMA((2,)),
            DMA((2,)),
            DMA,
            DMA,
            DMA,
            DMA((NY,)),
            DMA((NY,)),
        ],
        compiler_params=pltpu.CompilerParams(
            collective_id=1, has_side_effects=True, vmem_limit_bytes=32 << 20
        ),
        name="combine",
    )(hidden, down_w, stats)


ROWS = 16
HALF = 1024


def total_kernel(
    part_m, part_e, out_m, out_e, taken, chain_in, chain_out,
    give_sent, give_here, hop_sent, hop_here, ring_sent, ring_here,
    own_sent, own_here, rel_sent, rel_here,
):
    z, x, y, c = place()
    other = 1 - c
    sides = ((y + 1) % NY, (y + NY - 1) % NY)
    parts, outs = (part_m, part_e), (out_m, out_e)
    mine = pl.ds(pl.multiple_of(c * HALF, HALF), HALF)
    theirs = pl.ds(pl.multiple_of(other * HALF, HALF), HALF)
    barrier = pltpu.get_barrier_semaphore()
    greet(barrier, y=sides[0])
    greet(barrier, y=sides[1])
    greet(barrier, c=other)
    pl.semaphore_wait(barrier, 3)

    def away(m, way):
        return (y + m) % NY if way == 0 else (y + NY - m) % NY

    def gift(j):
        return put(
            parts[j].at[:, :, theirs], taken.at[j], give_sent.at[j], give_here.at[j], c=other
        )

    for j in range(2):
        gift(j).start()

    def own(j, dest):
        return parts[j][dest, :, mine].astype(jnp.float32) + taken[j, dest].astype(jnp.float32)

    def hop(m, j, way):
        return put(
            chain_out.at[way, m - 1, j], chain_in.at[way, m - 1, j],
            hop_sent.at[way, m - 1, j], hop_here.at[way, m - 1, j], y=sides[way],
        )

    for j in range(2):
        gift(j).wait_recv()
    for m in range(FAR, 0, -1):
        for j in range(2):
            for way in range(2):
                if m <= reach(way, j):
                    total = own(j, away(m, way))
                    if m < reach(way, j):
                        hop(m + 1, j, way).wait_recv()
                        total = total + chain_in[way, m, j].astype(jnp.float32)
                    chain_out[way, m - 1, j] = total.astype(jnp.bfloat16)
                    hop(m, j, way).start()

    def origin(k, way):
        return (y + NY - k) % NY if way == 0 else (y + k) % NY

    def ring(k, j, way):
        piece = outs[j].at[origin(k, way), :, mine]
        return put(piece, piece, ring_sent.at[way, k, j], ring_here.at[way, k, j], y=sides[way])

    def swap(j):
        piece = outs[j].at[y, :, mine]
        return put(piece, piece, own_sent.at[j], own_here.at[j], c=other)

    def relay(k, j, way):
        piece = outs[j].at[origin(k + 1, way), :, mine]
        return put(piece, piece, rel_sent.at[way, k, j], rel_here.at[way, k, j], c=other)

    for j in range(2):
        hop(1, j, 0).wait_recv()
        hop(1, j, 1).wait_recv()
        outs[j][y, :, mine] = (
            own(j, y)
            + chain_in[0, 0, j].astype(jnp.float32)
            + chain_in[1, 0, j].astype(jnp.float32)
        ).astype(jnp.bfloat16)
        for way in range(2):
            ring(0, j, way).start()
        swap(j).start()
    for k in range(FAR):
        for j in range(2):
            for way in range(2):
                if k < reach(way, j):
                    ring(k, j, way).wait_recv()
                    if k + 1 < reach(way, j):
                        ring(k + 1, j, way).start()
                    relay(k, j, way).start()
    for j in range(2):
        gift(j).wait_send()
        swap(j).wait()
        for k in range(FAR):
            for way in range(2):
                if k < reach(way, j):
                    hop(k + 1, j, way).wait_send()
                    ring(k, j, way).wait_send()
                    relay(k, j, way).wait()


def total_over_tp(part_m, part_e):
    shape = (NY, ROWS, 2048)
    out_m, out_e = pl.pallas_call(
        total_kernel,
        out_shape=(jax.ShapeDtypeStruct(shape, jnp.bfloat16),) * 2,
        in_specs=[VM, VM],
        out_specs=(VM, VM),
        scratch_shapes=[
            pltpu.VMEM((2, NY, ROWS, HALF), jnp.bfloat16),
            pltpu.VMEM((2, FAR, 2, ROWS, HALF), jnp.bfloat16),
            pltpu.VMEM((2, FAR, 2, ROWS, HALF), jnp.bfloat16),
            DMA((2,)),
            DMA((2,)),
            DMA((2, FAR, 2)),
            DMA((2, FAR, 2)),
            DMA((2, FAR, 2)),
            DMA((2, FAR, 2)),
            DMA((2,)),
            DMA((2,)),
            DMA((2, FAR, 2)),
            DMA((2, FAR, 2)),
        ],
        compiler_params=pltpu.CompilerParams(
            collective_id=2, has_side_effects=True, vmem_limit_bytes=16 << 20
        ),
        name="total",
    )(part_m.reshape(shape), part_e.reshape(shape))
    return out_m.reshape(-1, 2048), out_e.reshape(-1, 2048)


def row_norm(inputs, gains):
    widened = inputs.astype(jnp.float32)
    row_mean = jnp.mean(widened, axis=-1, keepdims=True)
    row_var = jnp.mean(jnp.square(widened - row_mean), axis=-1, keepdims=True)
    return (widened - row_mean) * lax.rsqrt(row_var + epsilon) * gains


def local(
    mixer_in,
    mixer_gain,
    w_value,
    w_gate,
    w_taps,
    channel_gain,
    w_output,
    expert_in,
    expert_gain,
    route_experts,
    route_scores,
    expert_gate,
    expert_up,
    expert_down,
):
    z, x, y, c = place()
    tokens = expert_in.shape[0]

    normed = row_norm(mixer_in, mixer_gain).astype(jnp.bfloat16)
    values = jnp.dot(normed, w_value, preferred_element_type=jnp.float32)
    gate_pre = jnp.dot(normed, w_gate, preferred_element_type=jnp.float32)
    gated_values = (values * jax.nn.sigmoid(gate_pre)).astype(jnp.bfloat16)
    channels = gated_values.shape[1]
    halo_in = jnp.pad(gated_values[tokens - 32 :], ((0, 0), (0, 128 - channels)))

    normed_b = row_norm(expert_in, expert_gain).astype(jnp.bfloat16)
    raised = jnp.exp(route_scores)
    route_weights = raised / jnp.sum(raised, axis=1, keepdims=True)
    served = []
    for j in range(2):
        dz, dx = shift_of(y, c, j)
        served.append(((z + dz) % NZ) * NX + (x + dx) % NX)
    served = jnp.stack(served).astype(jnp.int32)
    hits = route_experts[None, :, :] == served[:, None, None]
    named = jnp.any(hits, axis=2)
    earlier = jnp.arange(tokens)[:, None] < jnp.arange(tokens)[None, :]
    rank = jnp.dot(
        named.astype(jnp.bfloat16), earlier.astype(jnp.bfloat16), preferred_element_type=jnp.float32
    ).astype(jnp.int32)
    chosen = jnp.logical_and(
        named[:, None, :], rank[:, None, :] == jnp.arange(SLOTS, dtype=jnp.int32)[None, :, None]
    ).astype(jnp.bfloat16)
    send = (
        jnp.dot(chosen.reshape(2 * SLOTS, tokens), normed_b, preferred_element_type=jnp.float32)
        .astype(jnp.bfloat16)
        .reshape(2, SLOTS, -1)
    )

    hidden, halo = dispatch(send, halo_in, expert_gate, expert_up)

    first = jnp.logical_and(z == 0, x == 0)
    earlier_rows = jnp.where(first, jnp.zeros_like(halo), halo)[2:, :channels]
    extended = jnp.concatenate([earlier_rows, gated_values], axis=0)
    conv_out = jnp.zeros(gated_values.shape, jnp.float32)
    for offset in range(CONV_W):
        conv_out = (
            conv_out + extended[offset : offset + tokens].astype(jnp.float32) * w_taps[offset]
        )
    stats = jnp.concatenate(
        [
            jnp.sum(conv_out, axis=1)[None],
            jnp.sum(conv_out * conv_out, axis=1)[None],
            jnp.zeros((6, tokens), jnp.float32),
        ]
    )

    returned, stats = combine(hidden, expert_down, stats)

    row_mean = stats[0][:, None] / CONV_CH
    row_var = stats[1][:, None] / CONV_CH - row_mean * row_mean
    activated = jax.nn.silu(
        (conv_out - row_mean) * lax.rsqrt(row_var + epsilon) * channel_gain
    ).astype(jnp.bfloat16)
    part_m = jnp.dot(activated, w_output, preferred_element_type=jnp.float32).astype(jnp.bfloat16)

    weight = jnp.sum(jnp.where(hits, route_weights[None], 0.0), axis=2)
    part_e = jnp.zeros((tokens, returned.shape[2]), jnp.float32)
    for j in range(2):
        picked = lax.dot_general(
            chosen[j], returned[j], (((0,), (0,)), ((), ())), preferred_element_type=jnp.float32
        )
        part_e = part_e + picked * weight[j][:, None]
    return total_over_tp(part_m, part_e.astype(jnp.bfloat16))


def solution(mesh):
    split = Mesh(mesh.devices.reshape(NZ, NX, NY, 2), ("z", "x", "y", "c"))
    in_specs = (
        P(EP, None),
        P(),
        P(None, TP),
        P(None, TP),
        P(None, TP),
        P(TP),
        P(TP, None),
        P(EP, None),
        P(),
        P(EP, None),
        P(EP, None),
        P(EP, None, TP),
        P(EP, None, TP),
        P(EP, TP, None),
    )
    out_specs = (P(EP, None), P(EP, None))
    return jax.shard_map(local, mesh=split, in_specs=in_specs, out_specs=out_specs, check_vma=False)
```

time: 252 us -> 134 us (0.53)
  waiting for transfers between devices: 128 us -> 0 us
  Pallas kernels: 0 us -> 118 us
  blocking collectives: 56.2 us -> 0 us
  between operations: 15.5 us -> 1.04 us
  local copies, waits for them, and re-layouts: 20.4 us -> 7.59 us
  matrix products: 13.9 us -> 2.32 us
  other arithmetic: 13.6 us -> 3.47 us
  starting transfers between devices: 3.48 us -> 0 us
    pallas_call x0 -> x3, Pallas kernels: none -> 118 us  [the longest x1 46 us: dispatch(): pl.pallas_call(dispatch_kernel, out_shape=(jax.ShapeDtypeStruct((2, NY, 2...]
    all_gather x2 -> x0, waiting for transfers between devices: 74.9 us -> none  [the longest x1 42.1 us: local(): block_rows = lax.all_gather(arrived, TP, axis=0, tiled=True)]
    all_to_all x3 -> x0, blocking collectives: 56.2 us -> none  [the longest x1 24.8 us: local(): lax.all_to_all(sending, 'ep', split_axis=1, concat_axis=1, tiled=True)]
    reduce_scatter x1 -> x0, waiting for transfers between devices: 42.9 us -> none  [local(): lax.psum_scatter(jnp.dot(hidden, down_w, preferred_element_type=jnp.float...]
    dot_general x2 -> x4, matrix products: 11.9 us -> 1.21 us  [the longest x2 0.7 us: local(): lax.dot_general(chosen[j], returned[j], (((0,), (0,)), ((), ())), preferr...]
    gather x3 -> x0, local copies, waits for them, and re-layouts: 10.1 us -> none  [the longest x2 9.37 us: local(): picked = jnp.take(every_slot, slot_index * experts + flat_ids, axis=0)]
    psum x2 -> x0, waiting for transfers between devices: 9.51 us -> none  [by_axis(): x = lax.psum(x, axis)]
    reduce_sum x4 -> x2, other arithmetic: 7.42 us -> 0.46 us  [the longest x1 0.37 us: local(): jnp.sum(conv_out, axis=1)[None]]
  transfers between devices with their start and end apart: 6 -> 0, of which waited for: 5 -> 0; matrix products, arithmetic and copies ran while one was open for 9% -> 0% of each run, Pallas kernels for 0% -> 0%
where the time goes in v1:
time: 134 us; the launch traced here: 132 us
  Pallas kernels  118 us (88%)
  local copies, waits for them, and re-layouts  7.59 us (6%)
  other arithmetic  3.47 us (3%)
  matrix products  2.32 us (2%)
    pallas_call x1, Pallas kernels, dispatch(): pl.pallas_call(dispatch_kernel, out_shape=(jax.ShapeDtypeStruct((2, NY, 2...  46 us
    pallas_call x1, Pallas kernels, combine(): pl.pallas_call(combine_kernel, out_shape=(jax.ShapeDtypeStruct((2, SLOTS,...  40.4 us
    pallas_call x1, Pallas kernels, total_over_tp(): pl.pallas_call(total_kernel, out_shape=(jax.ShapeDtypeStruct(shape, jnp.b...  31.1 us
    unnamed x30, local copies, waits for them, and re-layouts  7.4 us

profile of v1, /device:TPU:1, one launch (start us, length us, event | category | flops | bytes accessed | tf_op | source)
XLA Modules:
  0.0 132.0 jit_solution(10257832098133104841)
XLA Ops:
  0.6 0.0 copy-start
  0.6 0.0 copy-start.4
  0.8 0.1 pad_add_fusion
  0.9 0.8 compare_reduce_fusion
  1.7 0.1 convolution_convert_fusion.2
  1.8 0.1 eq.62
  1.9 0.1 fusion.59
  2.0 1.2 convert_reduce_fusion.1
  3.2 0.0 copy-done.4
  3.2 0.0 copy-start.12
  3.2 0.3 fusion.14
  3.5 0.4 copy-done.12
  3.9 0.0 copy-start.5
  3.9 0.4 convolution_convert_fusion.1
  4.3 0.7 copy-done.5
  4.9 0.2 convert_reduce_fusion
  5.1 0.0 copy-start.10
  5.1 0.0 copy-start.13
  5.1 0.3 fusion.11
  5.4 0.7 copy-done.10
  6.1 0.0 copy-done.13
  6.1 0.0 copy-start.11
  6.1 0.4 fusion.65
  6.5 0.6 copy-done.11
  7.1 0.4 fusion.10
  7.5 0.6 copy-done.2
  8.1 0.2 copy-done.3
  8.3 46.0 %dispatch.1 = (bf16[2,8,64,128]{3,2,1,0:T(8,128)(2,1)S(1)}, bf16[32,128]{1,0:T(8,128)(2,1)S(1)}) custom-call(bf16[2,32,2048]{2,1,0:T(8,128)(2,1)S(1)} %bitcast.112, bf16[32,128]{1,0:T(8,128)(2,1)S(1)} %pad.4.halo_in, bf16[1,2048,128]{2,1,0:T(8,128)(2,1)S(1)} %copy-done.2, bf16[1,2048,128]{2,1,0:T(8,128)(2,1)S(1)} %copy-done.3), custom_call_target="tpu_custom_call" | custom-call | tf_op jit(solution)/shard_map/dispatch/pallas_call | solution.py:194
  54.3 0.0 copy-start.6
  54.3 0.7 copy-done.6
  55.0 0.4 fusion.67
  55.4 0.1 pad.7.clone
  55.5 0.1 maximum_maximum_fusion.stats
  55.6 0.0 copy-done.1
  55.6 40.4 %combine.1 = (bf16[2,32,2048]{2,1,0:T(8,128)(2,1)S(1)}, f32[8,128]{1,0:T(8,128)S(1)}) custom-call(bf16[2,8,64,128]{3,2,1,0:T(8,128)(2,1)S(1)} %get-tuple-element.9.hidden, bf16[1,128,2048]{2,1,0:T(8,128)(2,1)S(1)} %copy-done.1, f32[8,128]{1,0:T(8,128)S(1)} %maximum_maximum_fusion.stats), custom_call_target="tpu_custom_call" | custom-call | tf_op jit(solution)/shard_map/combine/pallas_call | solution.py:383
  96.0 0.0 copy-start.7
  96.0 0.7 copy-done.7
  96.7 0.7 copy-done.8
  97.4 0.1 fusion.60
  97.5 0.3 convolution_multiply_fusion.1
  97.8 0.4 fusion.1
  98.2 0.0 copy-start.9
  98.2 0.0 copy-done
  98.2 0.6 copy-done.9
  98.9 0.4 convolution_convert_fusion
  99.2 31.1 %total.1 = (bf16[8,16,2048]{2,1,0:T(8,128)(2,1)S(1)}, bf16[8,16,2048]{2,1,0:T(8,128)(2,1)S(1)}) custom-call(bf16[8,16,2048]{2,1,0:T(8,128)(2,1)S(1)} %bitcast.109, bf16[8,16,2048]{2,1,0:T(8,128)(2,1)S(1)} %bitcast.108), custom_call_target="tpu_custom_call" | custom-call | tf_op jit(solution)/shard_map/total/pallas_call | solution.py:521
  130.4 0.8 copy.29
  131.2 0.8 copy.30
  (21 shorter events, 0.1 us)
Async XLA Ops:
  0.6 97.6 %copy-start = (bf16[96,2048]{1,0:T(8,128)(2,1)S(1)}, bf16[96,2048]{1,0:T(8,128)(2,1)}, u32[]{:S(2)}) copy-start(bf16[96,2048]{1,0:T(8,128)(2,1)} %param.20) | copy-start | bytes 1179652
  0.6 2.5 %copy-start.4 = (bf16[128,2048]{1,0:T(8,128)(2,1)S(1)}, bf16[128,2048]{1,0:T(8,128)(2,1)}, u32[]{:S(2)}) copy-start(bf16[128,2048]{1,0:T(8,128)(2,1)} %param.21) | copy-start | bytes 1572868
  3.2 0.7 copy-start.12
  3.9 1.0 copy-start.5
  5.1 1.0 copy-start.10
  5.1 1.0 copy-start.13
  6.1 1.0 copy-start.11
  7.1 1.0 copy-start.2
  7.1 1.2 copy-start.3
  8.3 47.3 %copy-start.1 = (bf16[1,128,2048]{2,1,0:T(8,128)(2,1)S(1)}, bf16[1,128,2048]{2,1,0:T(8,128)(2,1)}, u32[]{:S(2)}) copy-start(bf16[1,128,2048]{2,1,0:T(8,128)(2,1)} %down.1) | copy-start | bytes 1572868
  54.3 0.7 copy-start.6
  96.0 0.7 copy-start.7
  96.7 0.7 copy-start.8
  98.2 0.7 copy-start.9

commit v2 on v0

v2 whole, which is shorter than its diff:
```python
from types import SimpleNamespace

import jax
import jax.numpy as jnp
from jax import lax
from jax.experimental import pallas as pl
from jax.experimental.pallas import tpu as pltpu
from jax.sharding import Mesh
from jax.sharding import PartitionSpec as P

CONV_CH = 1536
CONV_W = 31
EP = ("z", "x")
TP = ("y", "c")
NZ, NX, NY = 8, 4, 8
SLOTS = 32
NEAR = 8
HALF = 1024
FAR = NY // 2

epsilon = 1e-05
clamp_limit = 7.0
swish_slope = 1.702

VM = pl.BlockSpec(memory_space=pltpu.VMEM)
ANY = pl.BlockSpec(memory_space=pl.ANY)
DMA = pltpu.SemaphoreType.DMA


def far_shift(y, c):
    p = y // 4
    dz = (1 - p) * (3 + 2 * c) + p * (4 * (1 - c) + c * (6 - 4 * (y % 2)))
    return dz, y % 4


def near_shift(c, i):
    return (0, 1, NZ - 1, 2 + 4 * c)[i // 2], 2 * (i % 2) + c


def reach(way, j):
    return FAR if way == j else FAR - 1


def put(src, dst, sent, landed, **device):
    return pltpu.make_async_remote_copy(
        src_ref=src,
        dst_ref=dst,
        send_sem=sent,
        recv_sem=landed,
        device_id=device,
        device_id_type=pl.DeviceIdType.MESH,
    )


def place():
    return tuple(lax.axis_index(a) for a in ("z", "x", "y", "c"))


def tiles(count, width, body):
    def step(n, _):
        body(pl.ds(pl.multiple_of(n * width, width), width))
        return 0

    lax.fori_loop(0, count, step, 0)


def mm(a, b):
    return jnp.dot(a, b, preferred_element_type=jnp.float32)


def norm_into(out, inputs, gain):
    def rows(at):
        widened = inputs[at, :].astype(jnp.float32)
        mean = jnp.mean(widened, axis=-1, keepdims=True)
        centred = widened - mean
        var = jnp.mean(jnp.square(centred), axis=-1, keepdims=True)
        out[at, :] = (centred * lax.rsqrt(var + epsilon) * gain[...]).astype(jnp.bfloat16)

    tiles(4, 32, rows)


NAMES = []


def whole_kernel(*refs):
    r = SimpleNamespace(**dict(zip(NAMES, refs)))
    z, x, y, c = place()
    other = 1 - c
    sides = ((y + 1) % NY, (y + NY - 1) % NY)
    block = z * NX + x
    after = (block + 1) % (NZ * NX)
    before = (block + NZ * NX - 1) % (NZ * NX)
    bf16, f32 = jnp.bfloat16, jnp.float32

    def on(dz, dx):
        return dict(z=(z + dz) % NZ, x=(x + dx) % NX)

    def back(dz, dx):
        return dict(z=(z + NZ - dz) % NZ, x=(x + NX - dx) % NX)

    far = far_shift(y, c)
    near = [near_shift(c, i) for i in range(NEAR)]
    itself = c == 0
    not_itself = c == 1

    barrier = pltpu.get_barrier_semaphore()

    def greet(**device):
        pl.semaphore_signal(barrier, inc=1, device_id=device, device_id_type=pl.DeviceIdType.MESH)

    for n, shift in enumerate([far] + near):

        def both(shift=shift):
            greet(**on(*shift))
            greet(**back(*shift))

        if n == 1:
            pl.when(not_itself)(both)
        else:
            both()
    greet(c=other)
    for i in range(1, NY):
        greet(y=(y + i) % NY)
    greet(z=after // NX, x=after % NX)
    greet(z=before // NX, x=before % NX)
    load_sem = r.load_sem

    def load(n, src, dst):
        copy = pltpu.make_async_copy(src, dst, load_sem.at[n])
        copy.start()
        return copy

    load_tokens_b = load(0, r.expert_in, r.tokens_b)
    load_tokens_a = load(1, r.mixer_in, r.tokens_a)
    load_w_value = load(2, r.w_value_in, r.w_value)
    load_w_gate = load(3, r.w_gate_in, r.w_gate)
    load_gate = load(4, r.gate_in.at[0], r.weights.at[:, pl.ds(0, 128)])
    load_up = load(5, r.up_in.at[0], r.weights.at[:, pl.ds(128, 128)])
    load_down = load(6, r.down_in.at[0], r.down)
    load_w_output = load(7, r.w_output_in, r.w_output)

    routes = r.routes[...]
    raised = jnp.exp(r.scores[...])
    route_weights = raised / jnp.sum(raised, axis=0, keepdims=True)
    named, weight = [], []
    for shift in near + [far]:
        target = tuple(on(*shift).values())
        hit = routes == target[0] * NX + target[1]
        named.append(jnp.max(jnp.where(hit, 1.0, 0.0), axis=0, keepdims=True))
        weight.append(jnp.sum(jnp.where(hit, route_weights, 0.0), axis=0, keepdims=True))
    stacked = jnp.concatenate(named + [jnp.zeros((7, 128), f32)], axis=0).astype(bf16)
    sooner = lax.broadcasted_iota(jnp.int32, (128, 128), 0) < lax.broadcasted_iota(
        jnp.int32, (128, 128), 1
    )
    rank = mm(stacked, jnp.where(sooner, 1.0, 0.0).astype(bf16))
    slot = lax.broadcasted_iota(jnp.int32, (SLOTS, 128), 0).astype(f32)
    spread_weights = []
    for n in range(NEAR + 1):
        chosen = jnp.where(rank[n : n + 1] == slot, 1.0, 0.0) * named[n]
        r.pick[n * SLOTS : (n + 1) * SLOTS] = chosen.astype(bf16)
        spread_weights.append(chosen * weight[n])
    spread_weights.append(jnp.zeros((96, 128), f32))
    spread_weights = jnp.concatenate(spread_weights, axis=0)
    for n in range(3):
        turned = spread_weights[n * 128 : (n + 1) * 128].T
        high = turned.astype(bf16)
        r.back_high[n] = high
        r.back_low[n] = (turned - high.astype(f32)).astype(bf16)

    load_tokens_b.wait()
    norm_into(r.normed, r.tokens_b, r.expert_gain)
    normed = r.normed

    def far_columns(at):
        r.far_send[:, at] = mm(r.pick[NEAR * SLOTS :], normed[:, at]).astype(bf16)

    tiles(4, 512, far_columns)
    pl.semaphore_wait(barrier, jnp.where(itself, 26, 28))

    rows_far, rows_near = r.rows_far, r.rows_near

    def half(j):
        return pl.ds(16 * j, 16)

    def far_out(j):
        return put(
            r.far_send.at[half(j)], rows_far.at[y, c, half(j)],
            r.far_sent.at[j], r.far_here.at[j], **on(*far),
        )

    for j in range(2):
        far_out(j).start()

    def near_columns(at):
        r.near_send[:, :, at] = (
            mm(r.pick[: NEAR * SLOTS], normed[:, at]).astype(bf16).reshape(NEAR, SLOTS, 512)
        )

    tiles(4, 512, near_columns)

    def near_out(i):
        return put(
            r.near_send.at[i], rows_near.at[i, c],
            r.near_sent.at[i], r.near_here.at[i], **on(*near[i]),
        )

    stays_out = pltpu.make_async_copy(r.near_send.at[0], rows_near.at[0, c], r.stay_sem.at[0])

    def start_near(make, stay, i):
        if i == 0:
            pl.when(itself)(lambda: stay.start())
            pl.when(not_itself)(lambda: make(0).start())
        else:
            make(i).start()

    def wait_near(make, stay, i):
        if i == 0:
            pl.when(itself)(lambda: stay.wait())
            pl.when(not_itself)(lambda: make(0).wait())
        else:
            make(i).wait()

    for i in range(NEAR):
        start_near(near_out, stays_out, i)

    load_tokens_a.wait()
    norm_into(normed, r.tokens_a, r.mixer_gain)
    load_w_value.wait()
    load_w_gate.wait()
    values = mm(normed[...], r.w_value[...])
    gate_pre = mm(normed[...], r.w_gate[...])
    gated = (values * jax.nn.sigmoid(gate_pre)).astype(bf16)
    extended = r.extended
    extended[32:, :96] = gated.astype(f32)
    r.halo_out[...] = jnp.zeros((32, 128), bf16)
    r.halo_out[:, :96] = gated[96:]
    halo = put(
        r.halo_out, r.halo_in, r.halo_sem.at[0], r.halo_sem.at[1],
        z=after // NX, x=after % NX,
    )
    halo.start()

    def origin(k, way):
        return (y + NY - k) % NY if way == 0 else (y + k) % NY

    def ring(k, j, way):
        piece = rows_far.at[origin(k, way), c, half(j)]
        return put(
            piece, piece, r.ring_sent.at[way, k, j], r.ring_here.at[way, k, j], y=sides[way]
        )

    def relay(k, j, way):
        piece = rows_far.at[origin(k + 1, way), c, half(j)]
        return put(
            piece, piece, r.relay_sent.at[way, k, j], r.relay_here.at[way, k, j], c=other
        )

    def own(j):
        piece = rows_far.at[y, c, half(j)]
        return put(piece, piece, r.own_sent.at[j], r.own_here.at[j], c=other)

    def near_relay(i):
        piece = rows_near.at[i, c]
        return put(piece, piece, r.nrelay_sent.at[i], r.nrelay_here.at[i], c=other)

    def product(hidden, rows, at):
        both = mm(rows[at].reshape(2 * SLOTS, 2048), r.weights[...])
        gate = jnp.minimum(both[:, :128], clamp_limit)
        up = jnp.clip(both[:, 128:], -clamp_limit, clamp_limit)
        hidden[at] = (
            ((up + 1.0) * gate * jax.nn.sigmoid(swish_slope * gate))
            .astype(bf16)
            .reshape(2, SLOTS, 128)
        )

    hidden_far, hidden_near = r.hidden_far, r.hidden_near

    def near_in(i):
        wait_near(near_out, stays_out, i)
        near_relay(i).start()

    def near_product(i):
        near_relay(i).wait()
        product(hidden_near, rows_near, i)

    for j in range(2):
        far_out(j).wait()
        for way in range(2):
            ring(0, j, way).start()
        own(j).start()

    halo.wait()
    keep = jnp.where(block == 0, 0.0, 1.0)
    extended[:32, :96] = r.halo_in[:, :96].astype(f32) * keep
    conv = jnp.zeros((128, 96), f32)
    for tap in range(CONV_W):
        conv = conv + extended[2 + tap : 130 + tap, :96] * r.w_taps[tap : tap + 1, :]
    r.conv[...] = conv
    lane = lax.broadcasted_iota(jnp.int32, (128, 128), 1)
    sums = jnp.sum(conv, axis=1, keepdims=True)
    squares = jnp.sum(conv * conv, axis=1, keepdims=True)
    columns = jnp.where(lane == 0, sums, jnp.where(lane == 1, squares, 0.0))
    r.stats[...] = columns.T[:8]

    def stats_swap():
        return put(r.stats, r.stats_pair, r.swap_sem.at[0], r.swap_sem.at[1], c=other)

    def stats_spread(i):
        return put(
            r.stats_sum, r.stats_all.at[y], r.stats_sent.at[i], r.stats_here.at[i],
            y=(y + i) % NY,
        )

    stats_swap().start()
    load_gate.wait()
    load_up.wait()

    for k in range(FAR):
        for j in range(2):
            for way in range(2):
                if k < reach(way, j):
                    ring(k, j, way).wait_recv()
                    if k + 1 < reach(way, j):
                        ring(k + 1, j, way).start()
                    relay(k, j, way).start()
        if k == 0:
            own(0).wait()
            own(1).wait()
            product(hidden_far, rows_far, y)
            stats_swap().wait()
            r.stats_sum[...] = r.stats[...] + r.stats_pair[...]
            for i in range(1, NY):
                stats_spread(i).start()
        else:
            near_product(2 * k - 2)
            near_product(2 * k - 1)
        near_in(2 * k)
        near_in(2 * k + 1)
        for j in range(2):
            for way in range(2):
                if k < reach(way, j):
                    relay(k, j, way).wait_recv()
        for way in range(2 if k < FAR - 1 else 1):
            product(hidden_far, rows_far, origin(k + 1, way))

    def away(m, way):
        return (y + m) % NY if way == 0 else (y + NY - m) % NY

    order = [(FAR, 0)] + [(m, way) for m in range(FAR - 1, 0, -1) for way in range(2)] + [(0, 0)]
    mine, given, taken = r.mine, r.given, r.taken
    chain_in, chain_out = r.chain_in, r.chain_out
    load_down.wait()

    def gift(i):
        return put(given.at[i], taken.at[i], r.gift_sent.at[i], r.gift_here.at[i], c=other)

    def partial(i):
        dest = away(*order[i])

        def cols(at):
            mine[i, :, at] = mm(hidden_far[dest, c], r.down[:, at])
            given[i, :, at] = mm(hidden_far[dest, other], r.down[:, at]).astype(bf16)

        tiles(4, 512, cols)
        gift(i).start()

    def settle(i):
        gift(i).wait_recv()

    def chain(m, j, way):
        return put(
            chain_out.at[way, m - 1, j], chain_in.at[way, m - 1, j],
            r.chain_sent.at[way, m - 1, j], r.chain_here.at[way, m - 1, j], y=sides[way],
        )

    def so_far(i, j):
        return mine[i, 16 * j : 16 * j + 16] + taken[i, 16 * j : 16 * j + 16].astype(f32)

    def pass_on(m, j, way, i):
        total = so_far(i, j)
        if m < reach(way, j):
            chain(m + 1, j, way).wait_recv()
            total = total + chain_in[way, m, j].astype(f32)
        chain_out[way, m - 1, j] = total.astype(bf16)
        chain(m, j, way).start()

    def near_gift(b):
        at = pl.ds(4 * b, 4)
        return put(
            r.near_given.at[at], r.near_taken.at[at],
            r.ngift_sent.at[b], r.ngift_here.at[b], c=other,
        )

    def near_give():
        def cols(at):
            r.near_given[:, :, at] = (
                mm(hidden_near[:, other].reshape(NEAR * SLOTS, 128), r.down[:, at])
                .astype(bf16)
                .reshape(NEAR, SLOTS, 512)
            )

        tiles(4, 512, cols)
        near_gift(0).start()
        near_gift(1).start()

    def near_back(i):
        return put(
            r.near_ready.at[i], r.near_got.at[i],
            r.nback_sent.at[i], r.nback_here.at[i], **back(*near[i]),
        )

    stays_back = pltpu.make_async_copy(
        r.near_ready.at[0], r.near_got.at[0], r.stay_sem.at[1]
    )

    def near_return(b):
        near_gift(b).wait_recv()
        blocks = pl.ds(4 * b, 4)

        def cols(at):
            done = mm(hidden_near[blocks, c].reshape(4 * SLOTS, 128), r.down[:, at])
            r.near_ready[blocks, :, at] = (
                done.reshape(4, SLOTS, 512) + r.near_taken[blocks, :, at].astype(f32)
            ).astype(bf16)

        tiles(4, 512, cols)
        for i in range(4 * b, 4 * b + 4):
            start_near(near_back, stays_back, i)

    mine_at = pl.ds(pl.multiple_of(c * HALF, HALF), HALF)
    their_at = pl.ds(pl.multiple_of(other * HALF, HALF), HALF)
    outs = (r.out_m, r.out_e)
    rounds = (4, 3, 5, 2, 6, 1, 7)

    def part_gift(o):
        return put(
            r.part.at[o, :, :, their_at], r.part_taken.at[o],
            r.pgift_sent.at[o], r.pgift_here.at[o], c=other,
        )

    def scatter(o, i):
        return put(
            r.halves.at[o, (y + i) % NY], r.arrived.at[o, y],
            r.scat_sent.at[o, i], r.scat_here.at[o, i], y=(y + i) % NY,
        )

    def scatter_all(o):
        part_gift(o).wait_recv()
        r.halves[o] = (
            r.part[o, :, :, mine_at].astype(f32) + r.part_taken[o].astype(f32)
        ).astype(bf16)
        for i in rounds:
            scatter(o, i).start()

    def publish(o, i):
        piece = outs[o].at[y, :, mine_at]
        return put(
            piece, piece, r.pub_sent.at[o, i], r.pub_here.at[o, i], y=(y + i) % NY
        )

    def share(o, i):
        piece = outs[o].at[(y + NY - i) % NY, :, mine_at]
        return put(piece, piece, r.share_sent.at[o, i], r.share_here.at[o, i], c=other)

    def publish_all(o):
        total = r.part[o, y, :, mine_at].astype(f32) + r.part_taken[o, y].astype(f32)
        for i in reversed(rounds):
            scatter(o, i).wait_recv()
            total = total + r.arrived[o, (y + NY - i) % NY].astype(f32)
        outs[o][y, :, mine_at] = total.astype(bf16)
        for i in rounds:
            publish(o, i).start()
        share(o, 0).start()

    def share_all(o):
        for i in reversed(rounds):
            publish(o, i).wait_recv()
            share(o, i).start()

    def mixer_part():
        total = r.stats_sum[...]
        for i in range(1, NY):
            stats_spread(i).wait()
            total = total + r.stats_all[(y + NY - i) % NY]
        turned = jnp.concatenate([total, jnp.zeros((120, 128), f32)], axis=0).T
        row_mean = turned[:, 0:1] / CONV_CH
        row_var = turned[:, 1:2] / CONV_CH - row_mean * row_mean
        scaled = (r.conv[...] - row_mean) * lax.rsqrt(row_var + epsilon)
        scaled = scaled * r.channel_gain[...]
        activated = (scaled * jax.nn.sigmoid(scaled)).astype(bf16)
        load_w_output.wait()

        def cols(at):
            r.part[0, :, :, at] = (
                mm(activated, r.w_output[:, at]).astype(bf16).reshape(NY, 16, 512)
            )

        tiles(4, 512, cols)
        part_gift(0).start()

    partial(0)
    partial(1)
    partial(2)
    settle(0)
    pass_on(FAR, 0, 0, 0)
    pass_on(FAR, 1, 1, 0)
    for m in range(FAR - 1, 0, -1):
        i = 1 + 2 * (FAR - 1 - m)
        partial(i + 2)
        if m > 1:
            partial(i + 3)
        if m == 3:
            near_product(6)
            near_product(7)
        settle(i)
        settle(i + 1)
        for turn in range(2):
            for way in range(2):
                pass_on(m, 1 - way if turn == 0 else way, way, i + way)
        if m == 3:
            near_give()
            mixer_part()
        elif m == 2:
            near_return(0)
            scatter_all(0)
        else:
            near_return(1)
    last = len(order) - 1
    settle(last)

    def far_back(j):
        return put(
            r.far_ready.at[half(j)], r.far_got.at[half(j)],
            r.fback_sent.at[j], r.fback_here.at[j], **back(*far),
        )

    for j in range(2):
        chain(1, j, 0).wait_recv()
        chain(1, j, 1).wait_recv()
        r.far_ready[16 * j : 16 * j + 16] = (
            so_far(last, j) + chain_in[0, 0, j].astype(f32) + chain_in[1, 0, j].astype(f32)
        ).astype(bf16)
        far_back(j).start()

    publish_all(0)
    for i in range(NEAR):
        wait_near(near_back, stays_back, i)

    def near_sum(at):
        total = jnp.zeros((128, 512), f32)
        for n in range(2):
            got = r.near_got[4 * n : 4 * n + 4, :, at].reshape(128, 512)
            total = total + mm(r.back_high[n], got) + mm(r.back_low[n], got)
        r.summed[:, at] = total

    tiles(4, 512, near_sum)
    share_all(0)
    for j in range(2):
        far_back(j).wait()

    def far_sum(at):
        got = r.far_got[:, at]
        total = (
            r.summed[:, at]
            + mm(r.back_high[2, :, :SLOTS], got)
            + mm(r.back_low[2, :, :SLOTS], got)
        )
        r.part[1, :, :, at] = total.astype(bf16).reshape(NY, 16, 512)

    tiles(4, 512, far_sum)
    part_gift(1).start()
    scatter_all(1)
    publish_all(1)
    share_all(1)

    for j in range(2):
        for way in range(2):
            for k in range(reach(way, j)):
                ring(k, j, way).wait_send()
                relay(k, j, way).wait_send()
                chain(k + 1, j, way).wait_send()
    for i in range(len(order)):
        gift(i).wait_send()
    near_gift(0).wait_send()
    near_gift(1).wait_send()
    for o in range(2):
        part_gift(o).wait_send()
        share(o, 0).wait()
        for i in rounds:
            scatter(o, i).wait_send()
            publish(o, i).wait_send()
            share(o, i).wait()


def vm(*shape, dtype=jnp.bfloat16):
    return pltpu.VMEM(shape, dtype)


INPUTS = dict(
    mixer_in=ANY, mixer_gain=VM, w_value_in=ANY, w_gate_in=ANY, w_taps=VM,
    channel_gain=VM, w_output_in=ANY, expert_in=ANY, expert_gain=VM, routes=VM,
    scores=VM, gate_in=ANY, up_in=ANY, down_in=ANY,
)
F32 = jnp.float32
SCRATCH = dict(
    tokens_b=vm(128, 2048), tokens_a=vm(128, 2048), normed=vm(128, 2048),
    w_value=vm(2048, 96), w_gate=vm(2048, 96), weights=vm(2048, 256),
    down=vm(128, 2048), w_output=vm(96, 2048), pick=vm((NEAR + 1) * SLOTS, 128),
    back_high=vm(3, 128, 128), back_low=vm(3, 128, 128),
    far_send=vm(SLOTS, 2048), near_send=vm(NEAR, SLOTS, 2048),
    rows_far=vm(NY, 2, SLOTS, 2048), rows_near=vm(NEAR, 2, SLOTS, 2048),
    hidden_far=vm(NY, 2, SLOTS, 128), hidden_near=vm(NEAR, 2, SLOTS, 128),
    extended=vm(160, 128, dtype=F32), halo_out=vm(32, 128), halo_in=vm(32, 128),
    conv=vm(128, 96, dtype=F32), stats=vm(8, 128, dtype=F32),
    stats_pair=vm(8, 128, dtype=F32), stats_sum=vm(8, 128, dtype=F32),
    stats_all=vm(NY, 8, 128, dtype=F32), mine=vm(NY, SLOTS, 2048, dtype=F32),
    given=vm(NY, SLOTS, 2048), taken=vm(NY, SLOTS, 2048),
    chain_in=vm(2, FAR, 2, 16, 2048), chain_out=vm(2, FAR, 2, 16, 2048),
    near_given=vm(NEAR, SLOTS, 2048), near_taken=vm(NEAR, SLOTS, 2048),
    near_ready=vm(NEAR, SLOTS, 2048), near_got=vm(NEAR, SLOTS, 2048),
    far_ready=vm(SLOTS, 2048), far_got=vm(SLOTS, 2048), summed=vm(128, 2048, dtype=F32),
    part=vm(2, NY, 16, 2048), part_taken=vm(2, NY, 16, HALF), halves=vm(2, NY, 16, HALF),
    arrived=vm(2, NY, 16, HALF),
    load_sem=DMA((8,)), far_sent=DMA((2,)), far_here=DMA((2,)),
    near_sent=DMA((NEAR,)), near_here=DMA((NEAR,)), stay_sem=DMA((2,)),
    halo_sem=DMA((2,)), ring_sent=DMA((2, FAR, 2)), ring_here=DMA((2, FAR, 2)),
    relay_sent=DMA((2, FAR, 2)), relay_here=DMA((2, FAR, 2)), own_sent=DMA((2,)),
    own_here=DMA((2,)), nrelay_sent=DMA((NEAR,)), nrelay_here=DMA((NEAR,)),
    swap_sem=DMA((2,)), stats_sent=DMA((NY,)), stats_here=DMA((NY,)),
    gift_sent=DMA((NY,)), gift_here=DMA((NY,)), chain_sent=DMA((2, FAR, 2)),
    chain_here=DMA((2, FAR, 2)), ngift_sent=DMA((2,)), ngift_here=DMA((2,)),
    nback_sent=DMA((NEAR,)), nback_here=DMA((NEAR,)), fback_sent=DMA((2,)),
    fback_here=DMA((2,)), pgift_sent=DMA((2,)), pgift_here=DMA((2,)),
    scat_sent=DMA((2, NY)), scat_here=DMA((2, NY)), pub_sent=DMA((2, NY)),
    pub_here=DMA((2, NY)), share_sent=DMA((2, NY)), share_here=DMA((2, NY)),
)
NAMES += list(INPUTS | dict(out_m=VM, out_e=VM) | SCRATCH)


def local(
    mixer_in,
    mixer_gain,
    w_value,
    w_gate,
    w_taps,
    channel_gain,
    w_output,
    expert_in,
    expert_gain,
    route_experts,
    route_scores,
    expert_gate,
    expert_up,
    expert_down,
):
    shape = (NY, 16, 2048)
    out_m, out_e = pl.pallas_call(
        whole_kernel,
        out_shape=(jax.ShapeDtypeStruct(shape, jnp.bfloat16),) * 2,
        in_specs=list(INPUTS.values()),
        out_specs=(VM, VM),
        scratch_shapes=list(SCRATCH.values()),
        compiler_params=pltpu.CompilerParams(
            collective_id=0, has_side_effects=True, vmem_limit_bytes=48 << 20
        ),
        name="whole",
    )(
        mixer_in, mixer_gain[None], w_value, w_gate, w_taps, channel_gain[None], w_output,
        expert_in, expert_gain[None], route_experts.T, route_scores.T,
        expert_gate, expert_up, expert_down,
    )
    return out_m.reshape(-1, 2048), out_e.reshape(-1, 2048)


def solution(mesh):
    split = Mesh(mesh.devices.reshape(NZ, NX, NY, 2), ("z", "x", "y", "c"))
    in_specs = (
        P(EP, None),
        P(),
        P(None, TP),
        P(None, TP),
        P(None, TP),
        P(TP),
        P(TP, None),
        P(EP, None),
        P(),
        P(EP, None),
        P(EP, None),
        P(EP, None, TP),
        P(EP, None, TP),
        P(EP, TP, None),
    )
    out_specs = (P(EP, None), P(EP, None))
    return jax.shard_map(local, mesh=split, in_specs=in_specs, out_specs=out_specs, check_vma=False)
```

time: 252 us -> 111 us (0.44)
  waiting for transfers between devices: 128 us -> 0 us
  Pallas kernels: 0 us -> 103 us
  blocking collectives: 56.2 us -> 0 us
  between operations: 15.5 us -> 0.81 us
  matrix products: 13.9 us -> 0 us
  other arithmetic: 13.6 us -> 0 us
  local copies, waits for them, and re-layouts: 20.4 us -> 7.38 us
  starting transfers between devices: 3.48 us -> 0 us
    pallas_call x0 -> x1, Pallas kernels: none -> 103 us  [local(): pl.pallas_call(whole_kernel, out_shape=(jax.ShapeDtypeStruct(shape, jnp.b...]
    all_gather x2 -> x0, waiting for transfers between devices: 74.9 us -> none  [the longest x1 42.1 us: local(): block_rows = lax.all_gather(arrived, TP, axis=0, tiled=True)]
    all_to_all x3 -> x0, blocking collectives: 56.2 us -> none  [the longest x1 24.8 us: local(): lax.all_to_all(sending, 'ep', split_axis=1, concat_axis=1, tiled=True)]
    reduce_scatter x1 -> x0, waiting for transfers between devices: 42.9 us -> none  [local(): lax.psum_scatter(jnp.dot(hidden, down_w, preferred_element_type=jnp.float...]
    dot_general x5 -> x0, matrix products: 13.9 us -> none  [the longest x1 8.47 us: local(): jnp.dot(hidden, down_w, preferred_element_type=jnp.float32)]
    reduce_sum x9 -> x0, other arithmetic: 10.4 us -> none  [the longest x1 6.42 us: local(): jnp.sum(picked * route_weights[:, :, None], axis=1).astype(jnp.bfloat16)]
    gather x3 -> x0, local copies, waits for them, and re-layouts: 10.1 us -> none  [the longest x2 9.37 us: local(): picked = jnp.take(every_slot, slot_index * experts + flat_ids, axis=0)]
    psum x2 -> x0, waiting for transfers between devices: 9.51 us -> none  [by_axis(): x = lax.psum(x, axis)]
  transfers between devices with their start and end apart: 6 -> 0, of which waited for: 5 -> 0; matrix products, arithmetic and copies ran while one was open for 9% -> 0% of each run, Pallas kernels for 0% -> 0%
where the time goes in v2:
time: 111 us
  Pallas kernels  103 us (93%)
  local copies, waits for them, and re-layouts  7.38 us (7%)
    pallas_call x1, Pallas kernels, local(): pl.pallas_call(whole_kernel, out_shape=(jax.ShapeDtypeStruct(shape, jnp.b...  103 us
    unnamed x28, local copies, waits for them, and re-layouts  7.38 us

profile of v2, /device:TPU:1, one launch (start us, length us, event | category | flops | bytes accessed | tf_op | source)
XLA Modules:
  0.0 111.0 jit_solution(16553884867782354299)
XLA Ops:
  0.6 0.0 copy-start.1
  0.6 0.0 copy-start.2
  0.7 1.4 %copy.16.refs_2_ = bf16[2048,96]{1,0:T(8,128)(2,1)S(1)} copy(bf16[2048,96]{0,1:T(8,128)(2,1)} %param.16) | data formatting | bytes 786432 | tf_op args[2]
  2.0 0.0 copy-start
  2.0 0.0 copy-start.6
  2.0 0.0 copy-start.7
  2.0 0.0 copy-start.8
  2.1 0.0 copy-start.9
  2.1 0.0 copy-start.10
  2.1 0.0 copy-start.11
  2.1 1.3 %copy.17.refs_3_ = bf16[2048,96]{1,0:T(8,128)(2,1)S(1)} copy(bf16[2048,96]{0,1:T(8,128)(2,1)} %param.17) | data formatting | bytes 786432 | tf_op args[3]
  3.4 0.0 copy-done.1
  3.4 0.0 copy-done.2
  3.4 0.0 copy-done
  3.4 0.0 copy-done.6
  3.5 0.0 copy-done.7
  3.5 0.0 copy-done.8
  3.5 0.0 copy-done.9
  3.5 0.0 copy-done.10
  3.5 0.0 copy-done.11
  3.5 0.0 copy-start.3
  3.5 1.0 copy-done.3
  4.5 0.0 copy-start.4
  4.6 1.0 copy-done.4
  5.6 0.0 copy-start.5
  5.6 1.0 copy-done.5
  6.6 102.8 %whole.1 = (bf16[8,16,2048]{2,1,0:T(8,128)(2,1)S(1)}, bf16[8,16,2048]{2,1,0:T(8,128)(2,1)S(1)}) custom-call(bf16[128,2048]{1,0:T(8,128)(2,1)S(1)} %copy-done, f32[1,2048]{1,0:T(1,128)S(1)} %bitcast.9, bf16[2048,96]{1,0:T(8,128)(2,1)S(1)} %copy.16.refs_2_, bf16[2048,96]{1,0:T(8,128)(2,1)S(1)} %copy.17.refs_3_, f32[31,96]{1,0:T(8,128)S(1)} %copy-done.6, ...), custom_call_target="tpu_custom_call" | custom-call | tf_op jit(solution)/shard_map/whole/pallas_call | solution.py:657
  109.4 0.8 copy.20
  110.2 0.8 copy.21
Async XLA Ops:
  0.6 2.8 %copy-start.1 = (bf16[128,2048]{1,0:T(8,128)(2,1)S(1)}, bf16[128,2048]{1,0:T(8,128)(2,1)}, u32[]{:S(2)}) copy-start(bf16[128,2048]{1,0:T(8,128)(2,1)} %refs_7_.1) | copy-start | bytes 1572868
  0.6 2.8 %copy-start.2 = (bf16[1,2048,128]{2,1,0:T(8,128)(2,1)S(1)}, bf16[1,2048,128]{2,1,0:T(8,128)(2,1)}, u32[]{:S(2)}) copy-start(bf16[1,2048,128]{2,1,0:T(8,128)(2,1)} %refs_11_.1) | copy-start | bytes 1572868
  2.0 1.4 %copy-start = (bf16[128,2048]{1,0:T(8,128)(2,1)S(1)}, bf16[128,2048]{1,0:T(8,128)(2,1)}, u32[]{:S(2)}) copy-start(bf16[128,2048]{1,0:T(8,128)(2,1)} %refs_0_.1) | copy-start | bytes 1572868
  2.0 1.4 %copy-start.6 = (f32[31,96]{1,0:T(8,128)S(1)}, f32[31,96]{1,0:T(8,128)}, u32[]{:S(2)}) copy-start(f32[31,96]{1,0:T(8,128)} %refs_4_.1) | copy-start | bytes 35716
  2.0 1.4 %copy-start.7 = (f32[2048]{0:T(1024)S(1)}, f32[2048]{0:T(1024)}, u32[]{:S(2)}) copy-start(f32[2048]{0:T(1024)} %param.15) | copy-start | bytes 24580
  2.0 1.4 %copy-start.8 = (f32[2048]{0:T(1024)S(1)}, f32[2048]{0:T(1024)}, u32[]{:S(2)}) copy-start(f32[2048]{0:T(1024)} %param.22) | copy-start | bytes 24580
  2.1 1.4 %copy-start.9 = (s32[128,4]{0,1:T(4,128)S(1)}, s32[128,4]{0,1:T(4,128)}, u32[]{:S(2)}) copy-start(s32[128,4]{0,1:T(4,128)} %param.23) | copy-start | bytes 6148
  2.1 1.4 %copy-start.10 = (f32[128,4]{0,1:T(4,128)S(1)}, f32[128,4]{0,1:T(4,128)}, u32[]{:S(2)}) copy-start(f32[128,4]{0,1:T(4,128)} %param.24) | copy-start | bytes 6148
  2.1 1.4 %copy-start.11 = (f32[96]{0:T(128)S(1)}, f32[96]{0:T(128)}, u32[]{:S(2)}) copy-start(f32[96]{0:T(128)} %param.19) | copy-start | bytes 1156
  3.5 1.0 copy-start.3
  4.5 1.0 copy-start.4
  5.6 1.0 copy-start.5

commit v3 on v2

--- a/solution.py
+++ b/solution.py
@@ -191,44 +191,18 @@
     for j in range(2):
         far_out(j).start()
 
-    def near_columns(at):
-        r.near_send[:, :, at] = (
-            mm(r.pick[: NEAR * SLOTS], normed[:, at]).astype(bf16).reshape(NEAR, SLOTS, 512)
-        )
-
-    tiles(4, 512, near_columns)
-
-    def near_out(i):
-        return put(
-            r.near_send.at[i], rows_near.at[i, c],
-            r.near_sent.at[i], r.near_here.at[i], **on(*near[i]),
-        )
-
-    stays_out = pltpu.make_async_copy(r.near_send.at[0], rows_near.at[0, c], r.stay_sem.at[0])
-
-    def start_near(make, stay, i):
-        if i == 0:
-            pl.when(itself)(lambda: stay.start())
-            pl.when(not_itself)(lambda: make(0).start())
-        else:
-            make(i).start()
-
-    def wait_near(make, stay, i):
-        if i == 0:
-            pl.when(itself)(lambda: stay.wait())
-            pl.when(not_itself)(lambda: make(0).wait())
-        else:
-            make(i).wait()
-
-    for i in range(NEAR):
-        start_near(near_out, stays_out, i)
-
     load_tokens_a.wait()
-    norm_into(normed, r.tokens_a, r.mixer_gain)
+    norm_into(r.normed_a, r.tokens_a, r.mixer_gain)
     load_w_value.wait()
     load_w_gate.wait()
-    values = mm(normed[...], r.w_value[...])
-    gate_pre = mm(normed[...], r.w_gate[...])
+
+    def project(w):
+        return lax.dot_general(
+            r.normed_a[...], w[...], (((1,), (1,)), ((), ())), preferred_element_type=f32
+        )
+
+    values = project(r.w_value)
+    gate_pre = project(r.w_gate)
     gated = (values * jax.nn.sigmoid(gate_pre)).astype(bf16)
     extended = r.extended
     extended[32:, :96] = gated.astype(f32)
@@ -240,6 +214,38 @@
     )
     halo.start()
 
+    def near_columns(at):
+        r.near_send[:, :, at] = (
+            mm(r.pick[: NEAR * SLOTS], normed[:, at]).astype(bf16).reshape(NEAR, SLOTS, 512)
+        )
+
+    tiles(4, 512, near_columns)
+
+    def near_out(i):
+        return put(
+            r.near_send.at[i], rows_near.at[i, c],
+            r.near_sent.at[i], r.near_here.at[i], **on(*near[i]),
+        )
+
+    stays_out = pltpu.make_async_copy(r.near_send.at[0], rows_near.at[0, c], r.stay_sem.at[0])
+
+    def start_near(make, stay, i):
+        if i == 0:
+            pl.when(itself)(lambda: stay.start())
+            pl.when(not_itself)(lambda: make(0).start())
+        else:
+            make(i).start()
+
+    def wait_near(make, stay, i):
+        if i == 0:
+            pl.when(itself)(lambda: stay.wait())
+            pl.when(not_itself)(lambda: make(0).wait())
+        else:
+            make(i).wait()
+
+    for i in range(NEAR):
+        start_near(near_out, stays_out, i)
+
     def origin(k, way):
         return (y + NY - k) % NY if way == 0 else (y + k) % NY
 
@@ -263,109 +269,57 @@
         piece = rows_near.at[i, c]
         return put(piece, piece, r.nrelay_sent.at[i], r.nrelay_here.at[i], c=other)
 
-    def product(hidden, rows, at):
-        both = mm(rows[at].reshape(2 * SLOTS, 2048), r.weights[...])
+    hidden_far, hidden_near = r.hidden_far, r.hidden_near
+
+    def product(inputs):
+        both = mm(inputs, r.weights[...])
         gate = jnp.minimum(both[:, :128], clamp_limit)
         up = jnp.clip(both[:, 128:], -clamp_limit, clamp_limit)
-        hidden[at] = (
-            ((up + 1.0) * gate * jax.nn.sigmoid(swish_slope * gate))
-            .astype(bf16)
-            .reshape(2, SLOTS, 128)
-        )
-
-    hidden_far, hidden_near = r.hidden_far, r.hidden_near
+        return ((up + 1.0) * gate * jax.nn.sigmoid(swish_slope * gate)).astype(bf16)
+
+    def far_product(sources):
+        inputs = [rows_far[source].reshape(2 * SLOTS, 2048) for source in sources]
+        outputs = product(jnp.concatenate(inputs, axis=0) if len(inputs) > 1 else inputs[0])
+        for n, source in enumerate(sources):
+            hidden_far[source] = outputs[n * 64 : n * 64 + 64].reshape(2, SLOTS, 128)
 
     def near_in(i):
         wait_near(near_out, stays_out, i)
         near_relay(i).start()
 
-    def near_product(i):
-        near_relay(i).wait()
-        product(hidden_near, rows_near, i)
-
-    for j in range(2):
-        far_out(j).wait()
-        for way in range(2):
-            ring(0, j, way).start()
-        own(j).start()
-
-    halo.wait()
-    keep = jnp.where(block == 0, 0.0, 1.0)
-    extended[:32, :96] = r.halo_in[:, :96].astype(f32) * keep
-    conv = jnp.zeros((128, 96), f32)
-    for tap in range(CONV_W):
-        conv = conv + extended[2 + tap : 130 + tap, :96] * r.w_taps[tap : tap + 1, :]
-    r.conv[...] = conv
-    lane = lax.broadcasted_iota(jnp.int32, (128, 128), 1)
-    sums = jnp.sum(conv, axis=1, keepdims=True)
-    squares = jnp.sum(conv * conv, axis=1, keepdims=True)
-    columns = jnp.where(lane == 0, sums, jnp.where(lane == 1, squares, 0.0))
-    r.stats[...] = columns.T[:8]
-
-    def stats_swap():
-        return put(r.stats, r.stats_pair, r.swap_sem.at[0], r.swap_sem.at[1], c=other)
-
-    def stats_spread(i):
-        return put(
-            r.stats_sum, r.stats_all.at[y], r.stats_sent.at[i], r.stats_here.at[i],
-            y=(y + i) % NY,
-        )
-
-    stats_swap().start()
-    load_gate.wait()
-    load_up.wait()
-
-    for k in range(FAR):
-        for j in range(2):
-            for way in range(2):
-                if k < reach(way, j):
-                    ring(k, j, way).wait_recv()
-                    if k + 1 < reach(way, j):
-                        ring(k + 1, j, way).start()
-                    relay(k, j, way).start()
-        if k == 0:
-            own(0).wait()
-            own(1).wait()
-            product(hidden_far, rows_far, y)
-            stats_swap().wait()
-            r.stats_sum[...] = r.stats[...] + r.stats_pair[...]
-            for i in range(1, NY):
-                stats_spread(i).start()
-        else:
-            near_product(2 * k - 2)
-            near_product(2 * k - 1)
-        near_in(2 * k)
-        near_in(2 * k + 1)
-        for j in range(2):
-            for way in range(2):
-                if k < reach(way, j):
-                    relay(k, j, way).wait_recv()
-        for way in range(2 if k < FAR - 1 else 1):
-            product(hidden_far, rows_far, origin(k + 1, way))
+    def near_product(b):
+        for i in range(4 * b, 4 * b + 4):
+            near_relay(i).wait()
+        at = pl.ds(4 * b, 4)
+        hidden_near[at] = product(rows_near[at].reshape(8 * SLOTS, 2048)).reshape(4, 2, SLOTS, 128)
 
     def away(m, way):
         return (y + m) % NY if way == 0 else (y + NY - m) % NY
 
-    order = [(FAR, 0)] + [(m, way) for m in range(FAR - 1, 0, -1) for way in range(2)] + [(0, 0)]
     mine, given, taken = r.mine, r.given, r.taken
     chain_in, chain_out = r.chain_in, r.chain_out
-    load_down.wait()
-
-    def gift(i):
-        return put(given.at[i], taken.at[i], r.gift_sent.at[i], r.gift_here.at[i], c=other)
-
-    def partial(i):
-        dest = away(*order[i])
+
+    def first_of(m):
+        return 0 if m == FAR else 1 + 2 * (FAR - 1 - m)
+
+    def gift(m):
+        at = pl.ds(first_of(m), 1 if m in (0, FAR) else 2)
+        return put(given.at[at], taken.at[at], r.gift_sent.at[m], r.gift_here.at[m], c=other)
+
+    def partial(m):
+        dests = [away(m, way) for way in range(1 if m in (0, FAR) else 2)]
+        inputs = [hidden_far[dest, core] for core in (c, other) for dest in dests]
+        inputs = jnp.concatenate(inputs, axis=0)
+        count = len(dests)
+        at_m = pl.ds(first_of(m), count)
 
         def cols(at):
-            mine[i, :, at] = mm(hidden_far[dest, c], r.down[:, at])
-            given[i, :, at] = mm(hidden_far[dest, other], r.down[:, at]).astype(bf16)
+            done = mm(inputs, r.down[:, at]).reshape(2, count, SLOTS, 512)
+            mine[at_m, :, at] = done[0]
+            given[at_m, :, at] = done[1].astype(bf16)
 
         tiles(4, 512, cols)
-        gift(i).start()
-
-    def settle(i):
-        gift(i).wait_recv()
+        gift(m).start()
 
     def chain(m, j, way):
         return put(
@@ -376,8 +330,8 @@
     def so_far(i, j):
         return mine[i, 16 * j : 16 * j + 16] + taken[i, 16 * j : 16 * j + 16].astype(f32)
 
-    def pass_on(m, j, way, i):
-        total = so_far(i, j)
+    def pass_on(m, j, way):
+        total = so_far(first_of(m) + (0 if m == FAR else way), j)
         if m < reach(way, j):
             chain(m + 1, j, way).wait_recv()
             total = total + chain_in[way, m, j].astype(f32)
@@ -387,21 +341,19 @@
     def near_gift(b):
         at = pl.ds(4 * b, 4)
         return put(
-            r.near_given.at[at], r.near_taken.at[at],
-            r.ngift_sent.at[b], r.ngift_here.at[b], c=other,
-        )
-
-    def near_give():
+            r.near_given.at[at], r.near_taken.at[at], r.ngift_sent.at[b], r.ngift_here.at[b], c=other
+        )
+
+    def near_give(b):
+        blocks = pl.ds(4 * b, 4)
+        inputs = hidden_near[blocks, other].reshape(4 * SLOTS, 128)
+
         def cols(at):
-            r.near_given[:, :, at] = (
-                mm(hidden_near[:, other].reshape(NEAR * SLOTS, 128), r.down[:, at])
-                .astype(bf16)
-                .reshape(NEAR, SLOTS, 512)
-            )
+            done = mm(inputs, r.down[:, at]).astype(bf16)
+            r.near_given[blocks, :, at] = done.reshape(4, SLOTS, 512)
 
         tiles(4, 512, cols)
-        near_gift(0).start()
-        near_gift(1).start()
+        near_gift(b).start()
 
     def near_back(i):
         return put(
@@ -409,16 +361,15 @@
             r.nback_sent.at[i], r.nback_here.at[i], **back(*near[i]),
         )
 
-    stays_back = pltpu.make_async_copy(
-        r.near_ready.at[0], r.near_got.at[0], r.stay_sem.at[1]
-    )
+    stays_back = pltpu.make_async_copy(r.near_ready.at[0], r.near_got.at[0], r.stay_sem.at[1])
 
     def near_return(b):
         near_gift(b).wait_recv()
         blocks = pl.ds(4 * b, 4)
+        inputs = hidden_near[blocks, c].reshape(4 * SLOTS, 128)
 
         def cols(at):
-            done = mm(hidden_near[blocks, c].reshape(4 * SLOTS, 128), r.down[:, at])
+            done = mm(inputs, r.down[:, at])
             r.near_ready[blocks, :, at] = (
                 done.reshape(4, SLOTS, 512) + r.near_taken[blocks, :, at].astype(f32)
             ).astype(bf16)
@@ -438,19 +389,19 @@
             r.pgift_sent.at[o], r.pgift_here.at[o], c=other,
         )
 
-    def scatter(o, i):
-        return put(
-            r.halves.at[o, (y + i) % NY], r.arrived.at[o, y],
-            r.scat_sent.at[o, i], r.scat_here.at[o, i], y=(y + i) % NY,
-        )
-
-    def scatter_all(o):
-        part_gift(o).wait_recv()
-        r.halves[o] = (
-            r.part[o, :, :, mine_at].astype(f32) + r.part_taken[o].astype(f32)
+    def scatter(i):
+        return put(
+            r.halves.at[1, (y + i) % NY], r.arrived.at[y],
+            r.scat_sent.at[i], r.scat_here.at[i], y=(y + i) % NY,
+        )
+
+    def scatter_all():
+        part_gift(1).wait_recv()
+        r.halves[1] = (
+            r.part[1, :, :, mine_at].astype(f32) + r.part_taken[1].astype(f32)
         ).astype(bf16)
         for i in rounds:
-            scatter(o, i).start()
+            scatter(i).start()
 
     def publish(o, i):
         piece = outs[o].at[y, :, mine_at]
@@ -462,15 +413,15 @@
         piece = outs[o].at[(y + NY - i) % NY, :, mine_at]
         return put(piece, piece, r.share_sent.at[o, i], r.share_here.at[o, i], c=other)
 
-    def publish_all(o):
-        total = r.part[o, y, :, mine_at].astype(f32) + r.part_taken[o, y].astype(f32)
+    def publish_all():
+        total = r.part[1, y, :, mine_at].astype(f32) + r.part_taken[1, y].astype(f32)
         for i in reversed(rounds):
-            scatter(o, i).wait_recv()
-            total = total + r.arrived[o, (y + NY - i) % NY].astype(f32)
-        outs[o][y, :, mine_at] = total.astype(bf16)
+            scatter(i).wait_recv()
+            total = total + r.arrived[(y + NY - i) % NY].astype(f32)
+        outs[1][y, :, mine_at] = total.astype(bf16)
         for i in rounds:
-            publish(o, i).start()
-        share(o, 0).start()
+            publish(1, i).start()
+        share(1, 0).start()
 
     def share_all(o):
         for i in reversed(rounds):
@@ -498,35 +449,123 @@
         tiles(4, 512, cols)
         part_gift(0).start()
 
+    def mixer_own(dest, j):
+        at = slice(512 * j, 512 * j + 512)
+        return r.halves[0, dest, :, at].astype(f32)
+
+    def mixer_chain(m, j, way):
+        return put(
+            r.mchain_out.at[way, m - 1, j], r.mchain_in.at[way, m - 1, j],
+            r.mchain_sent.at[way, m - 1, j], r.mchain_here.at[way, m - 1, j], y=sides[way],
+        )
+
+    def mixer_pass(m, j, way):
+        total = mixer_own(away(m, way), j)
+        if m < reach(way, j):
+            mixer_chain(m + 1, j, way).wait_recv()
+            total = total + r.mchain_in[way, m, j].astype(f32)
+        r.mchain_out[way, m - 1, j] = total.astype(bf16)
+        mixer_chain(m, j, way).start()
+
+    def mixer_publish():
+        for j in range(2):
+            total = mixer_own(y, j)
+            for way in range(2):
+                mixer_chain(1, j, way).wait_recv()
+                total = total + r.mchain_in[way, 0, j].astype(f32)
+            r.out_m[y, :, pl.ds(pl.multiple_of(c * HALF + 512 * j, 512), 512)] = total.astype(bf16)
+        for i in rounds:
+            publish(0, i).start()
+        share(0, 0).start()
+
+    def conv_and_stats():
+        halo.wait()
+        keep = jnp.where(block == 0, 0.0, 1.0)
+        extended[:32, :96] = r.halo_in[:, :96].astype(f32) * keep
+        conv = jnp.zeros((128, 96), f32)
+        for tap in range(CONV_W):
+            conv = conv + extended[2 + tap : 130 + tap, :96] * r.w_taps[tap : tap + 1, :]
+        r.conv[...] = conv
+        lane = lax.broadcasted_iota(jnp.int32, (128, 128), 1)
+        sums = jnp.sum(conv, axis=1, keepdims=True)
+        squares = jnp.sum(conv * conv, axis=1, keepdims=True)
+        columns = jnp.where(lane == 0, sums, jnp.where(lane == 1, squares, 0.0))
+        r.stats[...] = columns.T[:8]
+        stats_swap().start()
+
+    def stats_spread(i):
+        return put(
+            r.stats_sum, r.stats_all.at[y], r.stats_sent.at[i], r.stats_here.at[i],
+            y=(y + i) % NY,
+        )
+
+    def stats_swap():
+        return put(r.stats, r.stats_pair, r.swap_sem.at[0], r.swap_sem.at[1], c=other)
+
+    load_gate.wait()
+    load_up.wait()
+    load_down.wait()
+    for j in range(2):
+        far_out(j).wait()
+        for way in range(2):
+            ring(0, j, way).start()
+        own(j).start()
+    conv_and_stats()
+    own(0).wait()
+    own(1).wait()
+    far_product([y])
     partial(0)
-    partial(1)
-    partial(2)
-    settle(0)
-    pass_on(FAR, 0, 0, 0)
-    pass_on(FAR, 1, 1, 0)
+    for k in range(FAR):
+        for j in range(2):
+            for way in range(2):
+                if k < reach(way, j):
+                    ring(k, j, way).wait_recv()
+                    if k + 1 < reach(way, j):
+                        ring(k + 1, j, way).start()
+                    relay(k, j, way).start()
+        near_in(2 * k)
+        near_in(2 * k + 1)
+        if k == 0:
+            stats_swap().wait()
+            r.stats_sum[...] = r.stats[...] + r.stats_pair[...]
+            for i in range(1, NY):
+                stats_spread(i).start()
+        elif k == 2:
+            near_product(0)
+        elif k == 3:
+            mixer_part()
+        for j in range(2):
+            for way in range(2):
+                if k < reach(way, j):
+                    relay(k, j, way).wait_recv()
+        far_product([origin(k + 1, way) for way in range(2 if k < FAR - 1 else 1)])
+        partial(k + 1)
+
+    gift(FAR).wait_recv()
+    pass_on(FAR, 0, 0)
+    pass_on(FAR, 1, 1)
+    part_gift(0).wait_recv()
+    r.halves[0] = (
+        r.part[0, :, :, mine_at].astype(f32) + r.part_taken[0].astype(f32)
+    ).astype(bf16)
+    mixer_pass(FAR, 0, 0)
+    mixer_pass(FAR, 1, 1)
+    near_give(0)
+    near_product(1)
     for m in range(FAR - 1, 0, -1):
-        i = 1 + 2 * (FAR - 1 - m)
-        partial(i + 2)
-        if m > 1:
-            partial(i + 3)
-        if m == 3:
-            near_product(6)
-            near_product(7)
-        settle(i)
-        settle(i + 1)
+        gift(m).wait_recv()
         for turn in range(2):
             for way in range(2):
-                pass_on(m, 1 - way if turn == 0 else way, way, i + way)
+                pass_on(m, 1 - way if turn == 0 else way, way)
+        for turn in range(2):
+            for way in range(2):
+                mixer_pass(m, 1 - way if turn == 0 else way, way)
         if m == 3:
-            near_give()
-            mixer_part()
+            near_return(0)
+            near_give(1)
         elif m == 2:
-            near_return(0)
-            scatter_all(0)
-        else:
             near_return(1)
-    last = len(order) - 1
-    settle(last)
+    gift(0).wait_recv()
 
     def far_back(j):
         return put(
@@ -538,11 +577,13 @@
         chain(1, j, 0).wait_recv()
         chain(1, j, 1).wait_recv()
         r.far_ready[16 * j : 16 * j + 16] = (
-            so_far(last, j) + chain_in[0, 0, j].astype(f32) + chain_in[1, 0, j].astype(f32)
+            so_far(first_of(0), j)
+            + chain_in[0, 0, j].astype(f32)
+            + chain_in[1, 0, j].astype(f32)
         ).astype(bf16)
         far_back(j).start()
 
-    publish_all(0)
+    mixer_publish()
     for i in range(NEAR):
         wait_near(near_back, stays_back, i)
 
@@ -569,8 +610,8 @@
 
     tiles(4, 512, far_sum)
     part_gift(1).start()
-    scatter_all(1)
-    publish_all(1)
+    scatter_all()
+    publish_all()
     share_all(1)
 
     for j in range(2):
@@ -579,15 +620,17 @@
                 ring(k, j, way).wait_send()
                 relay(k, j, way).wait_send()
                 chain(k + 1, j, way).wait_send()
-    for i in range(len(order)):
-        gift(i).wait_send()
+                mixer_chain(k + 1, j, way).wait_send()
+    for m in range(FAR + 1):
+        gift(m).wait_send()
     near_gift(0).wait_send()
     near_gift(1).wait_send()
+    for i in rounds:
+        scatter(i).wait_send()
     for o in range(2):
         part_gift(o).wait_send()
         share(o, 0).wait()
         for i in rounds:
-            scatter(o, i).wait_send()
             publish(o, i).wait_send()
             share(o, i).wait()
 
@@ -603,8 +646,8 @@
 )
 F32 = jnp.float32
 SCRATCH = dict(
-    tokens_b=vm(128, 2048), tokens_a=vm(128, 2048), normed=vm(128, 2048),
-    w_value=vm(2048, 96), w_gate=vm(2048, 96), weights=vm(2048, 256),
+    tokens_b=vm(128, 2048), tokens_a=vm(128, 2048), normed=vm(128, 2048), normed_a=vm(128, 2048),
+    w_value=vm(96, 2048), w_gate=vm(96, 2048), weights=vm(2048, 256),
     down=vm(128, 2048), w_output=vm(96, 2048), pick=vm((NEAR + 1) * SLOTS, 128),
     back_high=vm(3, 128, 128), back_low=vm(3, 128, 128),
     far_send=vm(SLOTS, 2048), near_send=vm(NEAR, SLOTS, 2048),
@@ -620,7 +663,7 @@
     near_ready=vm(NEAR, SLOTS, 2048), near_got=vm(NEAR, SLOTS, 2048),
     far_ready=vm(SLOTS, 2048), far_got=vm(SLOTS, 2048), summed=vm(128, 2048, dtype=F32),
     part=vm(2, NY, 16, 2048), part_taken=vm(2, NY, 16, HALF), halves=vm(2, NY, 16, HALF),
-    arrived=vm(2, NY, 16, HALF),
+    arrived=vm(NY, 16, HALF), mchain_in=vm(2, FAR, 2, 16, 512), mchain_out=vm(2, FAR, 2, 16, 512),
     load_sem=DMA((8,)), far_sent=DMA((2,)), far_here=DMA((2,)),
     near_sent=DMA((NEAR,)), near_here=DMA((NEAR,)), stay_sem=DMA((2,)),
     halo_sem=DMA((2,)), ring_sent=DMA((2, FAR, 2)), ring_here=DMA((2, FAR, 2)),
@@ -631,7 +674,7 @@
     chain_here=DMA((2, FAR, 2)), ngift_sent=DMA((2,)), ngift_here=DMA((2,)),
     nback_sent=DMA((NEAR,)), nback_here=DMA((NEAR,)), fback_sent=DMA((2,)),
     fback_here=DMA((2,)), pgift_sent=DMA((2,)), pgift_here=DMA((2,)),
-    scat_sent=DMA((2, NY)), scat_here=DMA((2, NY)), pub_sent=DMA((2, NY)),
+    scat_sent=DMA((NY,)), scat_here=DMA((NY,)), mchain_sent=DMA((2, FAR, 2)), mchain_here=DMA((2, FAR, 2)), pub_sent=DMA((2, NY)),
     pub_here=DMA((2, NY)), share_sent=DMA((2, NY)), share_here=DMA((2, NY)),
 )
 NAMES += list(INPUTS | dict(out_m=VM, out_e=VM) | SCRATCH)
@@ -661,11 +704,11 @@
         out_specs=(VM, VM),
         scratch_shapes=list(SCRATCH.values()),
         compiler_params=pltpu.CompilerParams(
-            collective_id=0, has_side_effects=True, vmem_limit_bytes=48 << 20
+            collective_id=0, has_side_effects=True, vmem_limit_bytes=58 << 20
         ),
         name="whole",
     )(
-        mixer_in, mixer_gain[None], w_value, w_gate, w_taps, channel_gain[None], w_output,
+        mixer_in, mixer_gain[None], w_value.T, w_gate.T, w_taps, channel_gain[None], w_output,
         expert_in, expert_gain[None], route_experts.T, route_scores.T,
         expert_gate, expert_up, expert_down,
     )

time: 111 us -> 98 us (0.88)
  Pallas kernels: 103 us -> 94.4 us
  local copies, waits for them, and re-layouts: 7.38 us -> 2.74 us
    pallas_call x1, Pallas kernels: 103 us -> 94.4 us  [local(): pl.pallas_call(whole_kernel, out_shape=(jax.ShapeDtypeStruct(shape, jnp.b...]
    unnamed x28 -> x4, local copies, waits for them, and re-layouts: 7.38 us -> 2.74 us
where the time goes in v3:
time: 98 us; the launch traced here: 97.8 us
  Pallas kernels  94.4 us (96%)
  local copies, waits for them, and re-layouts  2.74 us (3%)
    pallas_call x1, Pallas kernels, local(): pl.pallas_call(whole_kernel, out_shape=(jax.ShapeDtypeStruct(shape, jnp.b...  94.4 us
    unnamed x4, local copies, waits for them, and re-layouts  2.74 us

profile of v3, /device:TPU:1, one launch (start us, length us, event | category | flops | bytes accessed | tf_op | source)
XLA Modules:
  0.0 97.8 jit_solution(9566469136656583581)
XLA Ops:
  0.6 94.4 %whole.1 = (bf16[8,16,2048]{2,1,0:T(8,128)(2,1)}, bf16[8,16,2048]{2,1,0:T(8,128)(2,1)}) custom-call(bf16[128,2048]{1,0:T(8,128)(2,1)} %refs_0_.1, f32[1,2048]{1,0:T(1,128)} %bitcast.13, bf16[96,2048]{1,0:T(8,128)(2,1)} %bitcast.11, bf16[96,2048]{1,0:T(8,128)(2,1)} %bitcast.12, f32[31,96]{1,0:T(8,128)} %refs_4_.1, f32[1,96]{1,0:T(1,128)} %bitcast.17, ...), custom_call_target="tpu_custom_call" | custom-call | tf_op jit(solution)/shard_map/whole/pallas_call | solution.py:700
  95.1 0.0 copy-start
  95.1 1.9 %copy.18 = bf16[128,2048]{1,0:T(8,128)(2,1)} copy(bf16[128,2048]{1,0:T(8,128)(2,1)} %bitcast.10) | data formatting | bytes 1048576
  97.0 0.0 copy-done
  97.0 0.8 copy.19
Async XLA Ops:
  95.1 2.0 %copy-start = (bf16[8,16,2048]{2,1,0:T(8,128)(2,1)S(1)}, bf16[8,16,2048]{2,1,0:T(8,128)(2,1)}, u32[]{:S(2)}) copy-start(bf16[8,16,2048]{2,1,0:T(8,128)(2,1)} %get-tuple-element.5) | copy-start | bytes 1572868

commit v4 on v3

--- a/solution.py
+++ b/solution.py
@@ -15,6 +15,7 @@
 NZ, NX, NY = 8, 4, 8
 SLOTS = 32
 NEAR = 8
+ITSELF = 4
 HALF = 1024
 FAR = NY // 2
 
@@ -23,7 +24,7 @@
 swish_slope = 1.702
 
 VM = pl.BlockSpec(memory_space=pltpu.VMEM)
-ANY = pl.BlockSpec(memory_space=pl.ANY)
+HBM = pl.BlockSpec(memory_space=pltpu.HBM)
 DMA = pltpu.SemaphoreType.DMA
 
 
@@ -34,11 +35,15 @@
 
 
 def near_shift(c, i):
-    return (0, 1, NZ - 1, 2 + 4 * c)[i // 2], 2 * (i % 2) + c
+    return (1, NZ - 1, 0, 2 + 4 * c)[i // 2], 2 * (i % 2) + c
 
 
 def reach(way, j):
     return FAR if way == j else FAR - 1
+
+
+def piece_of(ref, p):
+    return ref.at[pl.ds(16 * (p // 2), 16), pl.ds(HALF * (p % 2), HALF)]
 
 
 def put(src, dst, sent, landed, **device):
@@ -103,6 +108,17 @@
     itself = c == 0
     not_itself = c == 1
 
+    load_sem = r.load_sem
+
+    def load(n, src, dst):
+        copy = pltpu.make_async_copy(src, dst, load_sem.at[n])
+        copy.start()
+        return copy
+
+    load_routes = load(0, r.routes_in, r.routes)
+    load_scores = load(1, r.scores_in, r.scores)
+    load_tokens_b = load(2, r.expert_in, r.tokens_b)
+    load_expert_gain = load(3, r.expert_gain_in, r.expert_gain)
     barrier = pltpu.get_barrier_semaphore()
 
     def greet(**device):
@@ -114,7 +130,7 @@
             greet(**on(*shift))
             greet(**back(*shift))
 
-        if n == 1:
+        if n == 1 + ITSELF:
             pl.when(not_itself)(both)
         else:
             both()
@@ -123,22 +139,19 @@
         greet(y=(y + i) % NY)
     greet(z=after // NX, x=after % NX)
     greet(z=before // NX, x=before % NX)
-    load_sem = r.load_sem
-
-    def load(n, src, dst):
-        copy = pltpu.make_async_copy(src, dst, load_sem.at[n])
-        copy.start()
-        return copy
-
-    load_tokens_b = load(0, r.expert_in, r.tokens_b)
-    load_tokens_a = load(1, r.mixer_in, r.tokens_a)
-    load_w_value = load(2, r.w_value_in, r.w_value)
-    load_w_gate = load(3, r.w_gate_in, r.w_gate)
-    load_gate = load(4, r.gate_in.at[0], r.weights.at[:, pl.ds(0, 128)])
-    load_up = load(5, r.up_in.at[0], r.weights.at[:, pl.ds(128, 128)])
-    load_down = load(6, r.down_in.at[0], r.down)
-    load_w_output = load(7, r.w_output_in, r.w_output)
-
+    load_tokens_a = load(4, r.mixer_in, r.tokens_a)
+    load_mixer_gain = load(5, r.mixer_gain_in, r.mixer_gain)
+    load_w_value = load(6, r.w_value_in, r.w_value)
+    load_w_gate = load(7, r.w_gate_in, r.w_gate)
+    load_w_taps = load(8, r.w_taps_in, r.w_taps)
+    load_gate = load(9, r.gate_in.at[0], r.weights.at[:, pl.ds(0, 128)])
+    load_up = load(10, r.up_in.at[0], r.weights.at[:, pl.ds(128, 128)])
+    load_down = load(11, r.down_in.at[0], r.down)
+    load_channel_gain = load(12, r.channel_gain_in, r.channel_gain)
+    load_w_output = load(13, r.w_output_in, r.w_output)
+
+    load_routes.wait()
+    load_scores.wait()
     routes = r.routes[...]
     raised = jnp.exp(r.scores[...])
     route_weights = raised / jnp.sum(raised, axis=0, keepdims=True)
@@ -168,6 +181,7 @@
         r.back_low[n] = (turned - high.astype(f32)).astype(bf16)
 
     load_tokens_b.wait()
+    load_expert_gain.wait()
     norm_into(r.normed, r.tokens_b, r.expert_gain)
     normed = r.normed
 
@@ -179,19 +193,17 @@
 
     rows_far, rows_near = r.rows_far, r.rows_near
 
-    def half(j):
-        return pl.ds(16 * j, 16)
-
-    def far_out(j):
-        return put(
-            r.far_send.at[half(j)], rows_far.at[y, c, half(j)],
-            r.far_sent.at[j], r.far_here.at[j], **on(*far),
-        )
-
-    for j in range(2):
-        far_out(j).start()
+    def far_out(p):
+        return put(
+            piece_of(r.far_send, p), piece_of(rows_far.at[y, c], p),
+            r.far_sent.at[p], r.far_here.at[p], **on(*far),
+        )
+
+    for p in range(4):
+        far_out(p).start()
 
     load_tokens_a.wait()
+    load_mixer_gain.wait()
     norm_into(r.normed_a, r.tokens_a, r.mixer_gain)
     load_w_value.wait()
     load_w_gate.wait()
@@ -227,19 +239,19 @@
             r.near_sent.at[i], r.near_here.at[i], **on(*near[i]),
         )
 
-    stays_out = pltpu.make_async_copy(r.near_send.at[0], rows_near.at[0, c], r.stay_sem.at[0])
+    stays_out = pltpu.make_async_copy(r.near_send.at[ITSELF], rows_near.at[ITSELF, c], r.stay_sem.at[0])
 
     def start_near(make, stay, i):
-        if i == 0:
+        if i == ITSELF:
             pl.when(itself)(lambda: stay.start())
-            pl.when(not_itself)(lambda: make(0).start())
+            pl.when(not_itself)(lambda: make(i).start())
         else:
             make(i).start()
 
     def wait_near(make, stay, i):
-        if i == 0:
+        if i == ITSELF:
             pl.when(itself)(lambda: stay.wait())
-            pl.when(not_itself)(lambda: make(0).wait())
+            pl.when(not_itself)(lambda: make(i).wait())
         else:
             make(i).wait()
 
@@ -249,21 +261,21 @@
     def origin(k, way):
         return (y + NY - k) % NY if way == 0 else (y + k) % NY
 
-    def ring(k, j, way):
-        piece = rows_far.at[origin(k, way), c, half(j)]
-        return put(
-            piece, piece, r.ring_sent.at[way, k, j], r.ring_here.at[way, k, j], y=sides[way]
-        )
-
-    def relay(k, j, way):
-        piece = rows_far.at[origin(k + 1, way), c, half(j)]
-        return put(
-            piece, piece, r.relay_sent.at[way, k, j], r.relay_here.at[way, k, j], c=other
-        )
-
-    def own(j):
-        piece = rows_far.at[y, c, half(j)]
-        return put(piece, piece, r.own_sent.at[j], r.own_here.at[j], c=other)
+    def ring(k, p, way):
+        piece = piece_of(rows_far.at[origin(k, way), c], p)
+        return put(
+            piece, piece, r.ring_sent.at[way, k, p], r.ring_here.at[way, k, p], y=sides[way]
+        )
+
+    def relay(k, p, way):
+        piece = piece_of(rows_far.at[origin(k + 1, way), c], p)
+        return put(
+            piece, piece, r.relay_sent.at[way, k, p], r.relay_here.at[way, k, p], c=other
+        )
+
+    def own(p):
+        piece = piece_of(rows_far.at[y, c], p)
+        return put(piece, piece, r.own_sent.at[p], r.own_here.at[p], c=other)
 
     def near_relay(i):
         piece = rows_near.at[i, c]
@@ -321,22 +333,27 @@
         tiles(4, 512, cols)
         gift(m).start()
 
-    def chain(m, j, way):
-        return put(
-            chain_out.at[way, m - 1, j], chain_in.at[way, m - 1, j],
-            r.chain_sent.at[way, m - 1, j], r.chain_here.at[way, m - 1, j], y=sides[way],
-        )
-
-    def so_far(i, j):
-        return mine[i, 16 * j : 16 * j + 16] + taken[i, 16 * j : 16 * j + 16].astype(f32)
-
-    def pass_on(m, j, way):
-        total = so_far(first_of(m) + (0 if m == FAR else way), j)
-        if m < reach(way, j):
-            chain(m + 1, j, way).wait_recv()
-            total = total + chain_in[way, m, j].astype(f32)
-        chain_out[way, m - 1, j] = total.astype(bf16)
-        chain(m, j, way).start()
+    def chain(m, p, way):
+        return put(
+            piece_of(chain_out.at[way, m - 1], p), piece_of(chain_in.at[way, m - 1], p),
+            r.chain_sent.at[way, m - 1, p], r.chain_here.at[way, m - 1, p], y=sides[way],
+        )
+
+    def span(p):
+        return slice(16 * (p // 2), 16 * (p // 2) + 16), slice(HALF * (p % 2), HALF * (p % 2) + HALF)
+
+    def so_far(i, p):
+        rows, cols = span(p)
+        return mine[i, rows, cols] + taken[i, rows, cols].astype(f32)
+
+    def pass_on(m, p, way):
+        rows, cols = span(p)
+        total = so_far(first_of(m) + (0 if m == FAR else way), p)
+        if m < reach(way, p // 2):
+            chain(m + 1, p, way).wait_recv()
+            total = total + chain_in[way, m, rows, cols].astype(f32)
+        chain_out[way, m - 1, rows, cols] = total.astype(bf16)
+        chain(m, p, way).start()
 
     def near_gift(b):
         at = pl.ds(4 * b, 4)
@@ -361,7 +378,7 @@
             r.nback_sent.at[i], r.nback_here.at[i], **back(*near[i]),
         )
 
-    stays_back = pltpu.make_async_copy(r.near_ready.at[0], r.near_got.at[0], r.stay_sem.at[1])
+    stays_back = pltpu.make_async_copy(r.near_ready.at[ITSELF], r.near_got.at[ITSELF], r.stay_sem.at[1])
 
     def near_return(b):
         near_gift(b).wait_recv()
@@ -429,6 +446,8 @@
             share(o, i).start()
 
     def mixer_part():
+        load_w_output.wait()
+        load_channel_gain.wait()
         total = r.stats_sum[...]
         for i in range(1, NY):
             stats_spread(i).wait()
@@ -439,7 +458,6 @@
         scaled = (r.conv[...] - row_mean) * lax.rsqrt(row_var + epsilon)
         scaled = scaled * r.channel_gain[...]
         activated = (scaled * jax.nn.sigmoid(scaled)).astype(bf16)
-        load_w_output.wait()
 
         def cols(at):
             r.part[0, :, :, at] = (
@@ -480,6 +498,7 @@
 
     def conv_and_stats():
         halo.wait()
+        load_w_taps.wait()
         keep = jnp.where(block == 0, 0.0, 1.0)
         extended[:32, :96] = r.halo_in[:, :96].astype(f32) * keep
         conv = jnp.zeros((128, 96), f32)
@@ -505,83 +524,87 @@
     load_gate.wait()
     load_up.wait()
     load_down.wait()
-    for j in range(2):
-        far_out(j).wait()
+    for p in range(4):
+        far_out(p).wait()
         for way in range(2):
-            ring(0, j, way).start()
-        own(j).start()
-    conv_and_stats()
-    own(0).wait()
-    own(1).wait()
-    far_product([y])
-    partial(0)
+            ring(0, p, way).start()
+        own(p).start()
     for k in range(FAR):
-        for j in range(2):
+        for p in range(4):
             for way in range(2):
-                if k < reach(way, j):
-                    ring(k, j, way).wait_recv()
-                    if k + 1 < reach(way, j):
-                        ring(k + 1, j, way).start()
-                    relay(k, j, way).start()
-        near_in(2 * k)
-        near_in(2 * k + 1)
+                if k < reach(way, p // 2):
+                    ring(k, p, way).wait_recv()
+                    if k + 1 < reach(way, p // 2):
+                        ring(k + 1, p, way).start()
+                    relay(k, p, way).start()
         if k == 0:
+            for p in range(4):
+                own(p).wait()
+            far_product([y])
+            conv_and_stats()
+        elif k == 1:
+            for i in range(4):
+                near_in(i)
             stats_swap().wait()
             r.stats_sum[...] = r.stats[...] + r.stats_pair[...]
             for i in range(1, NY):
                 stats_spread(i).start()
         elif k == 2:
+            for i in range(4, NEAR):
+                near_in(i)
             near_product(0)
-        elif k == 3:
+            near_give(0)
+        else:
             mixer_part()
-        for j in range(2):
+        for p in range(4):
             for way in range(2):
-                if k < reach(way, j):
-                    relay(k, j, way).wait_recv()
+                if k < reach(way, p // 2):
+                    relay(k, p, way).wait_recv()
         far_product([origin(k + 1, way) for way in range(2 if k < FAR - 1 else 1)])
         partial(k + 1)
 
     gift(FAR).wait_recv()
-    pass_on(FAR, 0, 0)
-    pass_on(FAR, 1, 1)
+    for p in range(4):
+        pass_on(FAR, p, p // 2)
     part_gift(0).wait_recv()
     r.halves[0] = (
         r.part[0, :, :, mine_at].astype(f32) + r.part_taken[0].astype(f32)
     ).astype(bf16)
     mixer_pass(FAR, 0, 0)
     mixer_pass(FAR, 1, 1)
-    near_give(0)
+    near_return(0)
     near_product(1)
+    near_give(1)
     for m in range(FAR - 1, 0, -1):
         gift(m).wait_recv()
         for turn in range(2):
-            for way in range(2):
-                pass_on(m, 1 - way if turn == 0 else way, way)
+            for q in range(2):
+                for way in range(2):
+                    pass_on(m, 2 * (1 - way if turn == 0 else way) + q, way)
         for turn in range(2):
             for way in range(2):
                 mixer_pass(m, 1 - way if turn == 0 else way, way)
         if m == 3:
-            near_return(0)
-            near_give(1)
-        elif m == 2:
             near_return(1)
+            partial(0)
     gift(0).wait_recv()
 
-    def far_back(j):
-        return put(
-            r.far_ready.at[half(j)], r.far_got.at[half(j)],
-            r.fback_sent.at[j], r.fback_here.at[j], **back(*far),
-        )
-
-    for j in range(2):
-        chain(1, j, 0).wait_recv()
-        chain(1, j, 1).wait_recv()
-        r.far_ready[16 * j : 16 * j + 16] = (
-            so_far(first_of(0), j)
-            + chain_in[0, 0, j].astype(f32)
-            + chain_in[1, 0, j].astype(f32)
+    def far_back(p):
+        return put(
+            piece_of(r.far_ready, p), piece_of(r.far_got, p),
+            r.fback_sent.at[p], r.fback_here.at[p], **back(*far),
+        )
+
+    for p in range(4):
+        rows, cols = span(p)
+        chain(1, p, 0).wait_recv()
+        chain(1, p, 1).wait_recv()
+        r.far_ready[rows, cols] = (
+            so_far(first_of(0), p)
+            + chain_in[0, 0, rows, cols].astype(f32)
+            + chain_in[1, 0, rows, cols].astype(f32)
         ).astype(bf16)
-        far_back(j).start()
+        far_back(p).start()
 
     mixer_publish()
     for i in range(NEAR):
@@ -595,9 +618,8 @@
         r.summed[:, at] = total
 
     tiles(4, 512, near_sum)
-    share_all(0)
-    for j in range(2):
-        far_back(j).wait()
+    for p in range(4):
+        far_back(p).wait()
 
     def far_sum(at):
         got = r.far_got[:, at]
@@ -611,16 +633,18 @@
     tiles(4, 512, far_sum)
     part_gift(1).start()
     scatter_all()
+    share_all(0)
     publish_all()
     share_all(1)
 
-    for j in range(2):
+    for p in range(4):
         for way in range(2):
-            for k in range(reach(way, j)):
-                ring(k, j, way).wait_send()
-                relay(k, j, way).wait_send()
-                chain(k + 1, j, way).wait_send()
-                mixer_chain(k + 1, j, way).wait_send()
+            for k in range(reach(way, p // 2)):
+                ring(k, p, way).wait_send()
+                relay(k, p, way).wait_send()
+                chain(k + 1, p, way).wait_send()
+                if p % 2 == 0:
+                    mixer_chain(k + 1, p // 2, way).wait_send()
     for m in range(FAR + 1):
         gift(m).wait_send()
     near_gift(0).wait_send()
@@ -640,12 +664,15 @@
 
 
 INPUTS = dict(
-    mixer_in=ANY, mixer_gain=VM, w_value_in=ANY, w_gate_in=ANY, w_taps=VM,
-    channel_gain=VM, w_output_in=ANY, expert_in=ANY, expert_gain=VM, routes=VM,
-    scores=VM, gate_in=ANY, up_in=ANY, down_in=ANY,
+    mixer_in=HBM, mixer_gain_in=HBM, w_value_in=HBM, w_gate_in=HBM, w_taps_in=HBM,
+    channel_gain_in=HBM, w_output_in=HBM, expert_in=HBM, expert_gain_in=HBM, routes_in=HBM,
+    scores_in=HBM, gate_in=HBM, up_in=HBM, down_in=HBM,
 )
 F32 = jnp.float32
 SCRATCH = dict(
+    mixer_gain=vm(1, 2048, dtype=F32), expert_gain=vm(1, 2048, dtype=F32),
+    w_taps=vm(31, 96, dtype=F32), channel_gain=vm(1, 96, dtype=F32),
+    routes=vm(4, 128, dtype=jnp.int32), scores=vm(4, 128, dtype=F32),
     tokens_b=vm(128, 2048), tokens_a=vm(128, 2048), normed=vm(128, 2048), normed_a=vm(128, 2048),
     w_value=vm(96, 2048), w_gate=vm(96, 2048), weights=vm(2048, 256),
     down=vm(128, 2048), w_output=vm(96, 2048), pick=vm((NEAR + 1) * SLOTS, 128),
@@ -658,22 +685,22 @@
     stats_pair=vm(8, 128, dtype=F32), stats_sum=vm(8, 128, dtype=F32),
     stats_all=vm(NY, 8, 128, dtype=F32), mine=vm(NY, SLOTS, 2048, dtype=F32),
     given=vm(NY, SLOTS, 2048), taken=vm(NY, SLOTS, 2048),
-    chain_in=vm(2, FAR, 2, 16, 2048), chain_out=vm(2, FAR, 2, 16, 2048),
+    chain_in=vm(2, FAR, SLOTS, 2048), chain_out=vm(2, FAR, SLOTS, 2048),
     near_given=vm(NEAR, SLOTS, 2048), near_taken=vm(NEAR, SLOTS, 2048),
     near_ready=vm(NEAR, SLOTS, 2048), near_got=vm(NEAR, SLOTS, 2048),
     far_ready=vm(SLOTS, 2048), far_got=vm(SLOTS, 2048), summed=vm(128, 2048, dtype=F32),
     part=vm(2, NY, 16, 2048), part_taken=vm(2, NY, 16, HALF), halves=vm(2, NY, 16, HALF),
     arrived=vm(NY, 16, HALF), mchain_in=vm(2, FAR, 2, 16, 512), mchain_out=vm(2, FAR, 2, 16, 512),
-    load_sem=DMA((8,)), far_sent=DMA((2,)), far_here=DMA((2,)),
+    load_sem=DMA((14,)), far_sent=DMA((4,)), far_here=DMA((4,)),
     near_sent=DMA((NEAR,)), near_here=DMA((NEAR,)), stay_sem=DMA((2,)),
-    halo_sem=DMA((2,)), ring_sent=DMA((2, FAR, 2)), ring_here=DMA((2, FAR, 2)),
-    relay_sent=DMA((2, FAR, 2)), relay_here=DMA((2, FAR, 2)), own_sent=DMA((2,)),
-    own_here=DMA((2,)), nrelay_sent=DMA((NEAR,)), nrelay_here=DMA((NEAR,)),
+    halo_sem=DMA((2,)), ring_sent=DMA((2, FAR, 4)), ring_here=DMA((2, FAR, 4)),
+    relay_sent=DMA((2, FAR, 4)), relay_here=DMA((2, FAR, 4)), own_sent=DMA((4,)),
+    own_here=DMA((4,)), nrelay_sent=DMA((NEAR,)), nrelay_here=DMA((NEAR,)),
     swap_sem=DMA((2,)), stats_sent=DMA((NY,)), stats_here=DMA((NY,)),
-    gift_sent=DMA((NY,)), gift_here=DMA((NY,)), chain_sent=DMA((2, FAR, 2)),
-    chain_here=DMA((2, FAR, 2)), ngift_sent=DMA((2,)), ngift_here=DMA((2,)),
-    nback_sent=DMA((NEAR,)), nback_here=DMA((NEAR,)), fback_sent=DMA((2,)),
-    fback_here=DMA((2,)), pgift_sent=DMA((2,)), pgift_here=DMA((2,)),
+    gift_sent=DMA((NY,)), gift_here=DMA((NY,)), chain_sent=DMA((2, FAR, 4)),
+    chain_here=DMA((2, FAR, 4)), ngift_sent=DMA((2,)), ngift_here=DMA((2,)),
+    nback_sent=DMA((NEAR,)), nback_here=DMA((NEAR,)), fback_sent=DMA((4,)),
+    fback_here=DMA((4,)), pgift_sent=DMA((2,)), pgift_here=DMA((2,)),
     scat_sent=DMA((NY,)), scat_here=DMA((NY,)), mchain_sent=DMA((2, FAR, 2)), mchain_here=DMA((2, FAR, 2)), pub_sent=DMA((2, NY)),
     pub_here=DMA((2, NY)), share_sent=DMA((2, NY)), share_here=DMA((2, NY)),
 )

time: 98 us -> 93.2 us (0.951)
  Pallas kernels: 94.4 us -> 89.7 us
    pallas_call x1, Pallas kernels: 94.4 us -> 89.7 us  [local(): pl.pallas_call(whole_kernel, out_shape=(jax.ShapeDtypeStruct(shape, jnp.b...]
where the time goes in v4:
time: 93.2 us; the launch traced here: 93.1 us
  Pallas kernels  89.7 us (96%)
  local copies, waits for them, and re-layouts  2.74 us (3%)
    pallas_call x1, Pallas kernels, local(): pl.pallas_call(whole_kernel, out_shape=(jax.ShapeDtypeStruct(shape, jnp.b...  89.7 us
    unnamed x4, local copies, waits for them, and re-layouts  2.74 us

profile of v4, /device:TPU:1, one launch (start us, length us, event | category | flops | bytes accessed | tf_op | source)
XLA Modules:
  0.0 93.1 jit_solution(15416634085589492460)
XLA Ops:
  0.6 89.7 %whole.1 = (bf16[8,16,2048]{2,1,0:T(8,128)(2,1)}, bf16[8,16,2048]{2,1,0:T(8,128)(2,1)}) custom-call(bf16[128,2048]{1,0:T(8,128)(2,1)} %refs_0_.1, f32[1,2048]{1,0:T(1,128)} %bitcast.13, bf16[96,2048]{1,0:T(8,128)(2,1)} %bitcast.11, bf16[96,2048]{1,0:T(8,128)(2,1)} %bitcast.12, f32[31,96]{1,0:T(8,128)} %refs_4_.1, f32[1,96]{1,0:T(1,128)} %bitcast.17, ...), custom_call_target="tpu_custom_call" | custom-call | tf_op jit(solution)/shard_map/whole/pallas_call | solution.py:727
  90.3 0.0 copy-start
  90.3 1.9 %copy.18 = bf16[128,2048]{1,0:T(8,128)(2,1)} copy(bf16[128,2048]{1,0:T(8,128)(2,1)} %bitcast.10) | data formatting | bytes 1048576
  92.3 0.0 copy-done
  92.3 0.8 copy.19
Async XLA Ops:
  90.3 2.0 %copy-start = (bf16[8,16,2048]{2,1,0:T(8,128)(2,1)S(1)}, bf16[8,16,2048]{2,1,0:T(8,128)(2,1)}, u32[]{:S(2)}) copy-start(bf16[8,16,2048]{2,1,0:T(8,128)(2,1)} %get-tuple-element.5) | copy-start | bytes 1572868
